TPU v7x, 32 devices: a whole 2x2x4 slice. The times are simulated.
32 devices in a mesh: rep: 2 (over y), fs: 4 (over z), tp: 4 (over x, core).
Axes of the slice: x: 2, y: 2, z: 4, core: 2. Of those that a mesh axis runs over, the one named last changes fastest.
Arguments:
- tokens: bfloat16 [2048, 2048], P(('rep', 'fs')), may hold values from -6 to 6
- norm_gains: float32 [3, 2048], replicated, may hold values from 0.1 to 1.9
- gate_weight: float32 [2048, 3072], P('fs', 'tp'), may hold values from -0.125 to 0.125
- up_weight: float32 [2048, 3072], P('fs', 'tp'), may hold values from -0.125 to 0.125
- hidden_scales: float32 [2, 3072], P(None, 'tp'), may hold values from 0.5 to 2
- down_weight: float32 [3072, 2048], P('tp', 'fs'), may hold values from -0.21875 to 0.21875
- down_scale: float32 [2048], P('fs'), may hold values from 0.5 to 2
- mix_in: float32 [2048, 512], P('fs'), may hold values from -0.125 to 0.125
- in_scale: float32 [512], replicated, may hold values from 0.5 to 2
- pool_map: float32 [4, 128, 128], replicated, may hold values from -0.5 to 0.5
- pool_scale: float32 [512], P('tp'), may hold values from 0.5 to 2
- mix_out: float32 [512, 2048], P('tp', 'fs'), may hold values from -0.25 to 0.25
- out_scale: float32 [2048], P('fs'), may hold values from 0.5 to 2
Outputs:
- layer_out: bfloat16 [2048, 2048], P(('rep', 'fs'))
All inputs are finite; a program needn't handle non-finite values.
Results may differ from a plain program's by a relative error of at most 0.02.
Values may be sent and summed in bfloat16 or wider, within the bound.
A program may use at most 64 MiB of HBM per device.

v0:
```python
import functools

import jax
import jax.numpy as jnp
from jax import lax
from jax.experimental import pallas as pl
from jax.experimental.pallas import tpu as pltpu
from jax.sharding import PartitionSpec as P

eps = 1e-06
widest = 16


def normed(values, gain):
    mean_sq = jnp.mean(values * values, axis=-1, keepdims=True)
    return (values * lax.rsqrt(mean_sq + eps) * gain).astype(jnp.bfloat16)


def scatter_rows(term_fn, share):
    return lax.psum_scatter(
        term_fn(jnp.int32(0), lax.axis_size("tp") * share).astype(jnp.bfloat16),
        "tp",
        scatter_dimension=0,
        tiled=True,
    ).astype(jnp.float32)


def whole_rows(values):
    return lax.all_gather(values, "tp", axis=0, tiled=True)


def fetch_mixer(in_cols, mix_out):
    return (
        lax.all_gather(in_cols.astype(jnp.bfloat16), "fs", axis=0, tiled=True),
        lax.all_gather(mix_out.astype(jnp.bfloat16), "fs", axis=1, tiled=True),
    )


def hidden_units(rows_in, gate_full, up_full, hidden_scales):
    gate = jnp.dot(rows_in, gate_full, preferred_element_type=jnp.float32) * hidden_scales[0]
    upper = jnp.dot(rows_in, up_full, preferred_element_type=jnp.float32) * hidden_scales[1]
    return (jax.nn.silu(gate) * upper).astype(jnp.bfloat16)


def ffn_partial(normed_rows, gate_full, up_full, down_full, hidden_scales, share):

    def term_rows(row_start, row_count):
        hidden = hidden_units(normed_rows, gate_full, up_full, hidden_scales)
        return jnp.dot(hidden, down_full, preferred_element_type=jnp.float32)

    return scatter_rows(term_rows, share)


def per_device(
    tokens,
    norm_gains,
    gate_weight,
    up_weight,
    hidden_scales,
    down_weight,
    down_scale,
    mix_in,
    in_scale,
    pool_map,
    pool_scale,
    mix_out,
    out_scale,
):
    tp_width = lax.axis_size("tp")
    tp_rank = lax.axis_index("tp")
    seq_rows = tokens.shape[0]
    share = seq_rows // tp_width
    local_channels = mix_out.shape[0]
    group_width = pool_map.shape[1]
    needed = max(group_width, local_channels)
    first_channel = tp_rank * local_channels
    in_start = first_channel // group_width * group_width
    in_cols = lax.dynamic_slice_in_dim(mix_in, in_start, needed, 1)
    scale_cols = lax.dynamic_slice_in_dim(in_scale, in_start, needed, 0)
    down_cols, out_cols = (
        lax.all_gather(down_scale, "fs", axis=0, tiled=True),
        lax.all_gather(out_scale, "fs", axis=0, tiled=True),
    )
    gate_bf = gate_weight.astype(jnp.bfloat16)
    up_bf = up_weight.astype(jnp.bfloat16)
    down_bf = down_weight.astype(jnp.bfloat16)
    resid_all = tokens.astype(jnp.float32)
    first = normed(resid_all, norm_gains[0])
    gate_full, up_full, down_full = (
        lax.all_gather(gate_bf, "fs", axis=0, tiled=True),
        lax.all_gather(up_bf, "fs", axis=0, tiled=True),
        lax.all_gather(down_bf, "fs", axis=1, tiled=True),
    )
    ffn_one = ffn_partial(first, gate_full, up_full, down_full, hidden_scales, share)
    own_rows = lax.dynamic_slice_in_dim(resid_all, tp_rank * share, share, 0)
    resid_one = own_rows + 0.5 * (ffn_one * down_cols)
    second = whole_rows(normed(resid_one, norm_gains[1]))
    in_full, out_full = fetch_mixer(in_cols, mix_out)
    pool_in = (jnp.dot(second, in_full, preferred_element_type=jnp.float32) * scale_cols).astype(
        jnp.bfloat16
    )
    channel = in_start + jnp.arange(needed, dtype=jnp.int32)
    window = jnp.left_shift(jnp.int32(2), channel // group_width)
    position = jnp.arange(seq_rows, dtype=jnp.int32)[:, None]
    values = pool_in.astype(jnp.float32)
    summed = jnp.zeros_like(values)
    for offset in range(widest):
        shifted = jnp.pad(values, ((offset, 0), (0, 0)))[:seq_rows]
        summed = summed + jnp.where(offset < window, shifted, 0.0)
    counts = jnp.minimum(position + 1, window).astype(jnp.float32)
    pooled = (summed / counts - values).astype(jnp.bfloat16)
    map_bf = pool_map.astype(jnp.bfloat16)
    if local_channels < group_width:
        group_index = first_channel // group_width
        column_start = first_channel % group_width
        map_cols = lax.dynamic_slice(
            map_bf, (group_index, jnp.int32(0), column_start), (1, group_width, local_channels)
        )[0]
        grouped = jnp.dot(pooled, map_cols, preferred_element_type=jnp.float32)
    else:
        held_groups = local_channels // group_width
        maps_held = lax.dynamic_slice_in_dim(map_bf, first_channel // group_width, held_groups, 0)
        grouped = jnp.einsum(
            "tgc,gcd->tgd",
            pooled.reshape(seq_rows, held_groups, group_width),
            maps_held,
            preferred_element_type=jnp.float32,
        ).reshape(seq_rows, local_channels)
    pool_out = (grouped * pool_scale).astype(jnp.bfloat16)

    def mixer_rows(row_start, row_count):
        return jnp.dot(pool_out, out_full, preferred_element_type=jnp.float32)

    mixed = scatter_rows(mixer_rows, share)
    resid_two = resid_one + mixed * out_cols
    third = whole_rows(normed(resid_two, norm_gains[2]))
    ffn_two = ffn_partial(third, gate_full, up_full, down_full, hidden_scales, share)
    final_rows = (resid_two + 0.5 * (ffn_two * down_cols)).astype(jnp.bfloat16)
    return whole_rows(final_rows)


MESH = pl.DeviceIdType.MESH
PARTS = (1, 1, 2, 4)
FIRST_PART = (0, 1, 2, 4, 8)
TILE = 256
bf16 = jnp.bfloat16
f32 = jnp.float32


def fits_kernel(mesh):
    return mesh.shape["rep"] == 2 and mesh.shape["fs"] == 4 and mesh.shape["tp"] == 4


def layer_kernel(
    n, tok, gains, gate_hbm, up_hbm, hs, down_hbm, mix_in_hbm, mix_out_hbm, isc, pmap, pool_scale, down_scale, out_scale,
    out, gu_in, dn_in, wi_in, wo_in, wide_gate, wide_up, wide_down, wide_in, wide_out, sc_in, ps_in, gu_buf, dn_buf, wi_all, wo_all, sc_all, ps_all,
    first, gacc, hidden, stage, rs, r1, second, pool, r2, third, rs_a, s_b, rs_b,
    ring_send, ring_recv, sc_send, sc_recv, tp_send, tp_recv, rs_send, rs_recv, ag_send, ag_recv, loc,
):
    rep, fs, me = lax.axis_index("rep"), lax.axis_index("fs"), lax.axis_index("tp")
    width = tok.shape[1]
    seq = tok.shape[0]
    slab = width // n
    share = seq // 4
    halo = widest
    units = hs.shape[1]
    gc = pmap.shape[1]
    core = me % 2
    mate = me + 1 - 2 * core
    across = (me + 2) % 4
    diag = (mate + 2) % 4
    peers = {1: mate, 2: across, 3: diag}

    order = (
        fs,
        jnp.where(fs == 0, 1, fs - 1),
        jnp.where(fs == 0, 2, jnp.where(fs == 1, 2, jnp.where(fs == 2, 3, 1))),
        jnp.where(fs < 2, 3, 0),
    )

    def owner_cols(i):
        return pl.ds(pl.multiple_of(order[i] * slab, slab), slab)

    def to_fs(offset):
        return {"fs": (fs + offset + n) % n}

    columns_in = pl.ds(pl.multiple_of(me * gc, gc), gc)
    half = slab // 2
    mine_half = pl.ds(pl.multiple_of(rep * half, half), half)
    other_half = pl.ds(pl.multiple_of((1 - rep) * half, half), half)
    loads = [
        pltpu.make_async_copy(mix_in_hbm.at[:, columns_in], wide_in, loc.at[2]),
        pltpu.make_async_copy(mix_out_hbm, wide_out, loc.at[3]),
        pltpu.make_async_copy(gate_hbm.at[mine_half, :], wide_gate.at[mine_half, :], loc.at[4]),
        pltpu.make_async_copy(up_hbm.at[mine_half, :], wide_up.at[mine_half, :], loc.at[5]),
        pltpu.make_async_copy(gate_hbm.at[other_half, :], wide_gate.at[other_half, :], loc.at[6]),
        pltpu.make_async_copy(up_hbm.at[other_half, :], wide_up.at[other_half, :], loc.at[7]),
        pltpu.make_async_copy(down_hbm, wide_down, loc.at[8]),
    ]
    for load in loads:
        load.start()
    barrier = pltpu.get_barrier_semaphore()
    for offset in range(1, n):
        pl.semaphore_signal(barrier, inc=1, device_id=to_fs(offset), device_id_type=MESH)
    for k in (1, 2, 3):
        pl.semaphore_signal(barrier, inc=1, device_id={"tp": peers[k]}, device_id_type=MESH)
    pl.semaphore_signal(barrier, inc=1, device_id={"rep": 1 - rep}, device_id_type=MESH)
    sc_in[...] = jnp.zeros_like(sc_in)
    sc_in[0:1, :] = down_scale[...]
    sc_in[1:2, :] = out_scale[...]
    ps_in[...] = jnp.broadcast_to(pool_scale[...], ps_in.shape)

    WI, WO, GU, DN = range(4)

    def slot(t, i):
        if t == WI:
            return wi_in if i == 0 else wi_all.at[0, order[i]]
        if t == WO:
            return wo_in if i == 0 else wo_all.at[0, order[i]]
        if t == GU:
            return gu_in if i == 0 else gu_buf.at[order[i]]
        return dn_in if i == 0 else dn_buf.at[order[i]]

    def there(t):
        return (wi_all.at[0], wo_all.at[0], gu_buf, dn_buf)[t]

    def part_of(ref, t, at):
        rows = ref.shape[0] // (2 * PARTS[t])
        return ref.at[pl.ds(pl.multiple_of(at * rows, rows), rows), :]

    started = []

    def start_if(cond, copy):
        if cond is None:
            copy.start()
        else:
            @pl.when(cond)
            def _():
                copy.start()
        started.append((cond, copy))

    def wait_sent():
        for cond, copy in started:
            if cond is None:
                copy.wait_send()
            else:
                @pl.when(cond)
                def _():
                    copy.wait_send()
        started.clear()

    UP, BACK, REP = range(3)

    def send(t, i, u, way):
        at = rep * PARTS[t] + u
        shard = order[i]
        dev = (to_fs(1), to_fs(-1), {"rep": 1 - rep})[way]
        cond = (fs < n - 1, fs > 0, None)[way]
        if i > 0 and way != REP:
            cond = cond & ((shard < fs) if way == UP else (shard > fs))
        start_if(cond, pltpu.make_async_remote_copy(
            src_ref=part_of(slot(t, i), t, at), dst_ref=part_of(there(t).at[shard], t, at),
            send_sem=ring_send.at[way, i, FIRST_PART[t] + u], recv_sem=ring_recv.at[shard, 2 * FIRST_PART[t] + at],
            device_id=dev, device_id_type=MESH,
        ))

    def arrived(t, i, at):
        here = part_of(slot(t, i), t, at)
        pltpu.make_async_remote_copy(
            src_ref=here, dst_ref=here, send_sem=ring_send.at[0, i, 0], recv_sem=ring_recv.at[order[i], 2 * FIRST_PART[t] + at],
            device_id={"rep": 1 - rep}, device_id_type=MESH,
        ).wait_recv()

    def remote(src, dst, s_sem, r_sem, dev):
        start_if(None, pltpu.make_async_remote_copy(
            src_ref=src, dst_ref=dst, send_sem=s_sem, recv_sem=r_sem, device_id=dev, device_id_type=MESH
        ))

    def landed(dst, s_sem, r_sem):
        pltpu.make_async_remote_copy(
            src_ref=dst, dst_ref=dst, send_sem=s_sem, recv_sem=r_sem, device_id={"tp": mate}, device_id_type=MESH
        ).wait_recv()

    def send_own(t):
        for u in range(PARTS[t]):
            send(t, 0, u, UP)
            send(t, 0, u, BACK)

    def relay(t, i):
        for u in range(PARTS[t]):
            arrived(t, i, rep * PARTS[t] + u)
            send(t, i, u, UP)
            send(t, i, u, BACK)
            send(t, i, u, REP)

    def rest(t, i):
        for u in range(PARTS[t]):
            arrived(t, i, (1 - rep) * PARTS[t] + u)

    loads[0].wait()
    loads[1].wait()
    wi_in[...] = wide_in[...].astype(bf16)
    wo_in[...] = wide_out[...].astype(bf16)
    def cast_gate_up(start, count):
        @pl.loop(0, count // 32)
        def _(j):
            rows = pl.ds(pl.multiple_of(start + j * 32, 32), 32)
            gu_in[rows, 0:units] = wide_gate[rows, :].astype(bf16)
            gu_in[rows, units:] = wide_up[rows, :].astype(bf16)

    pl.semaphore_wait(barrier, n - 1 + 4)
    send_own(WI)
    send_own(WO)
    loads[2].wait()
    loads[3].wait()
    for u in range(PARTS[GU]):
        cast_gate_up(rep * half + u * (half // PARTS[GU]), half // PARTS[GU])
        send(GU, 0, u, UP)
        send(GU, 0, u, BACK)

    def share_mixer(i):
        for t, held, own in ((0, wi_all, wi_in), (1, wo_all, wo_in)):
            src = own if i == 0 else held.at[0, order[i]]
            remote(src, held.at[2, order[i]], tp_send.at[t, i, 1], tp_recv.at[t, i, 1], {"tp": across})
            remote(src, held.at[1, order[i]], tp_send.at[t, i, 0], tp_recv.at[t, i, 0], {"tp": mate})

    def pass_mixer(i):
        for t, held in ((0, wi_all), (1, wo_all)):
            landed(held.at[2, order[i]], tp_send.at[t, i, 1], tp_recv.at[t, i, 1])
            remote(held.at[2, order[i]], held.at[3, order[i]], tp_send.at[t, i, 2], tp_recv.at[t, i, 2], {"tp": mate})

    share_mixer(0)
    loads[4].wait()
    loads[5].wait()
    cast_gate_up((1 - rep) * half, half)
    loads[6].wait()

    @pl.loop(0, units // 32)
    def _(j):
        rows = pl.ds(pl.multiple_of(j * 32, 32), 32)
        dn_in[rows, :] = wide_down[rows, :].astype(bf16)

    for offset in range(1, n):
        remote(sc_in, sc_all.at[fs], sc_send.at[offset - 1], sc_recv.at[fs], to_fs(offset))
    for k in (1, 2, 3):
        remote(ps_in, ps_all.at[k - 1], tp_send.at[2, 0, k - 1], tp_recv.at[2, 0, k - 1], {"tp": peers[k]})
    own_wi = pltpu.make_async_copy(wi_in, wi_all.at[0, fs], loc.at[0])
    own_wo = pltpu.make_async_copy(wo_in, wo_all.at[0, fs], loc.at[1])
    own_wi.start()
    own_wo.start()

    def normed_rows(values, gain):
        mean_sq = jnp.mean(values * values, axis=-1, keepdims=True)
        return (values * lax.rsqrt(mean_sq + eps) * gain).astype(bf16)

    stage[:, 0:halo, :] = jnp.zeros((n, halo, slab), bf16)

    @pl.loop(0, seq // 32)
    def _(i):
        rows = pl.ds(pl.multiple_of(i * 32, 32), 32)
        first[rows, :] = normed_rows(tok[rows, :].astype(f32), gains[0:1, :])

    def dot(a, b):
        return jnp.dot(a, b, preferred_element_type=f32)

    def gate_up(d, fresh):
        weights = slot(GU, d)
        cols = owner_cols(d)

        @pl.loop(0, weights.shape[1] // TILE)
        def _(j):
            at = pl.ds(pl.multiple_of(j * TILE, TILE), TILE)
            term = dot(first[:, cols], weights[:, at])
            if fresh:
                gacc[:, at] = term
            else:
                gacc[:, at] += term

    def activate(gate, upper, at):
        gate = gate * hs[0:1, at]
        upper = upper * hs[1:2, at]
        return (gate / (1.0 + jnp.exp(-gate)) * upper).astype(bf16)

    def down(d, top):
        weights = slot(DN, d)

        @pl.loop(0, slab // TILE)
        def _(j):
            at = pl.ds(pl.multiple_of(j * TILE, TILE), TILE)
            stage[d, top:top + seq, at] = dot(hidden[...], weights[:, at]).astype(bf16)

    gate_up(0, True)
    for t in (WI, WO, GU):
        relay(t, 1)
    send_own(DN)
    for t in (WI, WO, GU):
        relay(t, 2)
    rest(WI, 1)
    rest(WO, 1)
    share_mixer(1)
    rest(GU, 1)
    gate_up(1, False)
    for t in (WI, WO, GU):
        relay(t, 3)
    pass_mixer(0)
    rest(WI, 2)
    rest(WO, 2)
    share_mixer(2)
    rest(GU, 2)
    gate_up(2, False)
    rest(WI, 3)
    rest(WO, 3)
    share_mixer(3)
    own_wi.wait()
    own_wo.wait()
    pass_mixer(1)
    relay(DN, 1)
    rest(GU, 3)
    gate_up(3, False)

    @pl.loop(0, units // TILE)
    def _(j):
        at = pl.ds(pl.multiple_of(j * TILE, TILE), TILE)
        up_at = pl.ds(pl.multiple_of(units + j * TILE, TILE), TILE)
        hidden[:, at] = activate(gacc[:, at], gacc[:, up_at], at)

    def scatter_one(d):
        down(d, halo)
        for k in (2, 3, 1):
            rows = pl.ds(pl.multiple_of(peers[k] * share, share), share + halo)
            remote(stage.at[d, rows, :], rs.at[d, k - 1], rs_send.at[d, k - 1], rs_recv.at[d, k - 1], {"tp": peers[k]})

    for i in range(1, n):
        landed(sc_all.at[order[i]], sc_send.at[0], sc_recv.at[order[i]])

    def scales(d):
        return sc_in if d == 0 else sc_all.at[order[d]]

    own_window = pl.ds(pl.multiple_of(me * share, share), share + halo)
    own_rows = pl.ds(pl.multiple_of(me * share, share), share)
    before = pl.ds(pl.multiple_of((me * share + seq - halo) % seq, halo), halo)

    def gather_one(d):
        total = stage[d, own_window, :].astype(f32)
        for k in (1, 2, 3):
            landed(rs.at[d, k - 1], rs_send.at[d, k - 1], rs_recv.at[d, k - 1])
            total = total + rs[d, k - 1].astype(f32)
        total = 0.5 * (total * scales(d)[0:1, :])
        cols = owner_cols(d)
        r1[0:halo, cols] = total[0:halo] + jnp.where(me > 0, tok[before, cols].astype(f32), 0.0)
        r1[halo:, cols] = total[halo:] + tok[own_rows, cols].astype(f32)

    scatter_one(0)
    relay(DN, 2)
    pass_mixer(2)
    rest(DN, 1)
    scatter_one(1)
    gather_one(0)
    relay(DN, 3)
    pass_mixer(3)
    rest(DN, 2)
    scatter_one(2)
    gather_one(1)
    rest(DN, 3)
    scatter_one(3)
    gather_one(2)
    for k in (1, 2, 3):
        landed(ps_all.at[k - 1], tp_send.at[2, 0, k - 1], tp_recv.at[2, 0, k - 1])
    for i in range(n):
        for t, held in ((0, wi_all), (1, wo_all)):
            landed(held.at[1, order[i]], tp_send.at[t, i, 0], tp_recv.at[t, i, 0])
            landed(held.at[3, order[i]], tp_send.at[t, i, 2], tp_recv.at[t, i, 2])
    gather_one(3)

    second[...] = normed_rows(r1[...], gains[1:2, :])
    for k in range(4):
        group = me if k == 0 else peers[k]
        total = dot(second[:, owner_cols(0)], wi_all[k, fs])
        for d in range(1, n):
            total = total + dot(second[:, owner_cols(d)], wi_all[k, order[d]])
        values = (total * isc[pl.ds(group, 1), :]).astype(bf16).astype(f32)
        sum2 = values + pltpu.roll(values, 1, 0)
        sum4 = sum2 + pltpu.roll(sum2, 2, 0)
        sum8 = sum4 + pltpu.roll(sum4, 4, 0)
        sum16 = sum8 + pltpu.roll(sum8, 8, 0)
        summed = jnp.where(group == 0, sum2, jnp.where(group == 1, sum4, jnp.where(group == 2, sum8, sum16)))
        span = jnp.where(group == 0, 2, jnp.where(group == 1, 4, jnp.where(group == 2, 8, 16)))
        position = lax.broadcasted_iota(jnp.int32, (share, gc), 0) + me * share
        counts = jnp.minimum(position + 1, span).astype(f32)
        pooled = (summed[halo:] / counts - values[halo:]).astype(bf16)
        pscale = (ps_in if k == 0 else ps_all.at[k - 1])[0:1, :]
        pool[k] = (dot(pooled, pmap[group].astype(bf16)) * pscale).astype(bf16)
    for d in range(n):
        cols = owner_cols(d)
        total = dot(pool[0], wo_all[0, order[d]])
        for k in range(1, 4):
            total = total + dot(pool[k], wo_all[k, order[d]])
        r2[:, cols] = r1[halo:, cols] + total * scales(d)[1:2, :]
    third[own_rows, :] = normed_rows(r2[...], gains[2:3, :])

    def rows_of(rank, count=1):
        return pl.ds(pl.multiple_of(rank * share, share), share * count)

    def gather_rows(ref, cols, s):
        mine = ref.at[rows_of(me), cols]
        remote(mine, mine, ag_send.at[s, 1], ag_recv.at[s, 1], {"tp": across})
        remote(mine, mine, ag_send.at[s, 0], ag_recv.at[s, 0], {"tp": mate})

    def forward_rows(ref, cols, s):
        theirs = ref.at[rows_of(across), cols]
        landed(theirs, ag_send.at[s, 1], ag_recv.at[s, 1])
        remote(theirs, theirs, ag_send.at[s, 2], ag_recv.at[s, 2], {"tp": mate})

    everything = slice(None)
    gather_rows(third, everything, n)
    landed(third.at[rows_of(mate), :], ag_send.at[n, 0], ag_recv.at[n, 0])

    def hidden_half(chip):
        rows = rows_of(2 * chip, 2)

        @pl.loop(0, units // TILE)
        def _(j):
            at = pl.ds(pl.multiple_of(j * TILE, TILE), TILE)
            up_at = pl.ds(pl.multiple_of(units + j * TILE, TILE), TILE)
            gate = upper = None
            for d in range(n):
                weights = slot(GU, d)
                left = third[rows, owner_cols(d)]
                g, u = dot(left, weights[:, at]), dot(left, weights[:, up_at])
                gate, upper = (g, u) if gate is None else (gate + g, upper + u)
            hidden[rows, at] = activate(gate, upper, at)

    wait_sent()
    forward_rows(third, everything, n)
    hidden_half(me // 2)
    landed(third.at[rows_of(diag), :], ag_send.at[n, 2], ag_recv.at[n, 2])
    hidden_half(1 - me // 2)
    for d in range(n):
        down(d, 0)
        remote(stage.at[d, rows_of(diag), :], rs_a.at[d, 1], rs_send.at[n + d, 1], rs_recv.at[n + d, 1], {"tp": mate})
        remote(stage.at[d, rows_of(mate), :], rs_a.at[d, 0], rs_send.at[n + d, 0], rs_recv.at[n + d, 0], {"tp": mate})
    for d in range(n):
        landed(rs_a.at[d, 1], rs_send.at[n + d, 1], rs_recv.at[n + d, 1])
        s_b[d] = (stage[d, rows_of(across), :].astype(f32) + rs_a[d, 1].astype(f32)).astype(bf16)
        remote(s_b.at[d], rs_b.at[d], rs_send.at[n + d, 2], rs_recv.at[n + d, 2], {"tp": across})
    for d in range(n):
        landed(rs_a.at[d, 0], rs_send.at[n + d, 0], rs_recv.at[n + d, 0])
        landed(rs_b.at[d], rs_send.at[n + d, 2], rs_recv.at[n + d, 2])
        total = stage[d, rows_of(me), :].astype(f32) + rs_a[d, 0].astype(f32) + rs_b[d].astype(f32)
        cols = owner_cols(d)
        out[rows_of(me), cols] = (r2[:, cols] + 0.5 * (total * scales(d)[0:1, :])).astype(bf16)
        gather_rows(out, cols, d)
    for d in range(n):
        forward_rows(out, owner_cols(d), d)
    for d in range(n):
        landed(out.at[rows_of(mate), owner_cols(d)], ag_send.at[d, 0], ag_recv.at[d, 0])
        landed(out.at[rows_of(diag), owner_cols(d)], ag_send.at[d, 2], ag_recv.at[d, 2])
    wait_sent()


def fused_layer(
    tokens, norm_gains, gate_weight, up_weight, hidden_scales, down_weight, down_scale, mix_in, in_scale,
    pool_map, pool_scale, mix_out, out_scale,
):
    n = lax.axis_size("fs")
    seq, width = tokens.shape
    slab, units = gate_weight.shape
    groups, gc, _ = pool_map.shape
    share = seq // 4
    padded = share + widest
    vmem = pl.BlockSpec(memory_space=pltpu.VMEM)
    dma = pltpu.SemaphoreType.DMA
    hbm = pl.BlockSpec(memory_space=pl.ANY)
    args = (
        (tokens, vmem), (norm_gains, vmem), (gate_weight, hbm), (up_weight, hbm), (hidden_scales, vmem),
        (down_weight, hbm), (mix_in, hbm), (mix_out, hbm), (in_scale.reshape(groups, gc), vmem), (pool_map, vmem),
        (pool_scale[None], vmem), (down_scale[None], vmem), (out_scale[None], vmem),
    )
    return pl.pallas_call(
        functools.partial(layer_kernel, n),
        out_shape=jax.ShapeDtypeStruct((seq, width), bf16),
        in_specs=[spec for _, spec in args],
        out_specs=vmem,
        scratch_shapes=[
            pltpu.VMEM((slab, 2 * units), bf16),
            pltpu.VMEM((units, slab), bf16),
            pltpu.VMEM((slab, gc), bf16),
            pltpu.VMEM((gc, slab), bf16),
            pltpu.VMEM((slab, units), f32),
            pltpu.VMEM((slab, units), f32),
            pltpu.VMEM((units, slab), f32),
            pltpu.VMEM((slab, gc), f32),
            pltpu.VMEM((gc, slab), f32),
            pltpu.VMEM((8, slab), f32),
            pltpu.VMEM((8, gc), f32),
            pltpu.VMEM((n, slab, 2 * units), bf16),
            pltpu.VMEM((n, units, slab), bf16),
            pltpu.VMEM((4, n, slab, gc), bf16),
            pltpu.VMEM((4, n, gc, slab), bf16),
            pltpu.VMEM((n, 8, slab), f32),
            pltpu.VMEM((3, 8, gc), f32),
            pltpu.VMEM((seq, width), bf16),
            pltpu.VMEM((seq, 2 * units), f32),
            pltpu.VMEM((seq, units), bf16),
            pltpu.VMEM((n, seq + widest, slab), bf16),
            pltpu.VMEM((n, 3, padded, slab), bf16),
            pltpu.VMEM((padded, width), f32),
            pltpu.VMEM((padded, width), bf16),
            pltpu.VMEM((4, share, gc), bf16),
            pltpu.VMEM((share, width), f32),
            pltpu.VMEM((seq, width), bf16),
            pltpu.VMEM((n, 2, share, slab), bf16),
            pltpu.VMEM((n, share, slab), bf16),
            pltpu.VMEM((n, share, slab), bf16),
            dma((3, n, FIRST_PART[-1])), dma((n, 2 * FIRST_PART[-1])),
            dma((n - 1,)), dma((n,)),
            dma((3, n, 3)), dma((3, n, 3)),
            dma((2 * n, 3)), dma((2 * n, 3)),
            dma((n + 1, 3)), dma((n + 1, 3)),
            dma((9,)),
        ],
        compiler_params=pltpu.CompilerParams(
            collective_id=0, has_side_effects=True, vmem_limit_bytes=60 * 1024 * 1024
        ),
    )(*[value for value, _ in args])


def solution(mesh):
    body = fused_layer if fits_kernel(mesh) else per_device
    return jax.shard_map(
        body,
        mesh=mesh,
        in_specs=(
            P(("rep", "fs"), None),
            P(),
            P("fs", "tp"),
            P("fs", "tp"),
            P(None, "tp"),
            P("tp", "fs"),
            P("fs"),
            P("fs", None),
            P(),
            P(),
            P("tp"),
            P("tp", "fs"),
            P("fs"),
        ),
        out_specs=P(("rep", "fs"), None),
        check_vma=False,
    )
```

profile of v0, /device:TPU:1, one launch (start us, length us, event | category | flops | bytes accessed | tf_op | source)
XLA Modules:
  0.0 150.8 jit_solution(6847956184937494918)
XLA Ops:
  0.0 148.5 %shard_map.127 = bf16[256,2048]{1,0:T(8,128)(2,1)} custom-call(bf16[256,2048]{1,0:T(8,128)(2,1)} %tok.1, f32[3,2048]{1,0:T(4,128)} %gains.1, f32[512,768]{1,0:T(8,128)} %gate_hbm.1, f32[512,768]{1,0:T(8,128)} %up_hbm.1, f32[2,768]{1,0:T(2,128)} %hs.1, f32[768,512]{1,0:T(8,128)} %down_hbm.1, f32[512,512]{1,0:T(8,128)} %mix_in_hbm.1, f32[128,512]{1,0:T(8,128)} %mix_out_hbm.1, ...), custom_call_target="tpu_custom_call" | custom-call | tf_op jit(solution)/shard_map/pallas_call | solution.py:579
  148.5 2.3 %copy.15 = bf16[256,2048]{1,0:T(8,128)(2,1)} copy(bf16[256,2048]{1,0:T(8,128)(2,1)} %shard_map.127) | data formatting | bytes 2097152
where the time goes:
time: 151 us
  Pallas kernels  148 us (98%)
  local copies, waits for them, and re-layouts  2.3 us (2%)
    pallas_call x1, Pallas kernels, fused_layer(): pl.pallas_call(functools.partial(layer_kernel, n), out_shape=jax.ShapeDty...  148 us

commit v1 on v0

v1 whole, which is shorter than its diff:
```python
import functools

import jax
import jax.numpy as jnp
from jax import lax
from jax.experimental import pallas as pl
from jax.experimental.pallas import tpu as pltpu
from jax.sharding import PartitionSpec as P

eps = 1e-06
widest = 16


def normed(values, gain):
    mean_sq = jnp.mean(values * values, axis=-1, keepdims=True)
    return (values * lax.rsqrt(mean_sq + eps) * gain).astype(jnp.bfloat16)


def scatter_rows(term_fn, share):
    return lax.psum_scatter(
        term_fn(jnp.int32(0), lax.axis_size("tp") * share).astype(jnp.bfloat16),
        "tp",
        scatter_dimension=0,
        tiled=True,
    ).astype(jnp.float32)


def whole_rows(values):
    return lax.all_gather(values, "tp", axis=0, tiled=True)


def fetch_mixer(in_cols, mix_out):
    return (
        lax.all_gather(in_cols.astype(jnp.bfloat16), "fs", axis=0, tiled=True),
        lax.all_gather(mix_out.astype(jnp.bfloat16), "fs", axis=1, tiled=True),
    )


def hidden_units(rows_in, gate_full, up_full, hidden_scales):
    gate = jnp.dot(rows_in, gate_full, preferred_element_type=jnp.float32) * hidden_scales[0]
    upper = jnp.dot(rows_in, up_full, preferred_element_type=jnp.float32) * hidden_scales[1]
    return (jax.nn.silu(gate) * upper).astype(jnp.bfloat16)


def ffn_partial(normed_rows, gate_full, up_full, down_full, hidden_scales, share):

    def term_rows(row_start, row_count):
        hidden = hidden_units(normed_rows, gate_full, up_full, hidden_scales)
        return jnp.dot(hidden, down_full, preferred_element_type=jnp.float32)

    return scatter_rows(term_rows, share)


def per_device(
    tokens,
    norm_gains,
    gate_weight,
    up_weight,
    hidden_scales,
    down_weight,
    down_scale,
    mix_in,
    in_scale,
    pool_map,
    pool_scale,
    mix_out,
    out_scale,
):
    tp_width = lax.axis_size("tp")
    tp_rank = lax.axis_index("tp")
    seq_rows = tokens.shape[0]
    share = seq_rows // tp_width
    local_channels = mix_out.shape[0]
    group_width = pool_map.shape[1]
    needed = max(group_width, local_channels)
    first_channel = tp_rank * local_channels
    in_start = first_channel // group_width * group_width
    in_cols = lax.dynamic_slice_in_dim(mix_in, in_start, needed, 1)
    scale_cols = lax.dynamic_slice_in_dim(in_scale, in_start, needed, 0)
    down_cols, out_cols = (
        lax.all_gather(down_scale, "fs", axis=0, tiled=True),
        lax.all_gather(out_scale, "fs", axis=0, tiled=True),
    )
    gate_bf = gate_weight.astype(jnp.bfloat16)
    up_bf = up_weight.astype(jnp.bfloat16)
    down_bf = down_weight.astype(jnp.bfloat16)
    resid_all = tokens.astype(jnp.float32)
    first = normed(resid_all, norm_gains[0])
    gate_full, up_full, down_full = (
        lax.all_gather(gate_bf, "fs", axis=0, tiled=True),
        lax.all_gather(up_bf, "fs", axis=0, tiled=True),
        lax.all_gather(down_bf, "fs", axis=1, tiled=True),
    )
    ffn_one = ffn_partial(first, gate_full, up_full, down_full, hidden_scales, share)
    own_rows = lax.dynamic_slice_in_dim(resid_all, tp_rank * share, share, 0)
    resid_one = own_rows + 0.5 * (ffn_one * down_cols)
    second = whole_rows(normed(resid_one, norm_gains[1]))
    in_full, out_full = fetch_mixer(in_cols, mix_out)
    pool_in = (jnp.dot(second, in_full, preferred_element_type=jnp.float32) * scale_cols).astype(
        jnp.bfloat16
    )
    channel = in_start + jnp.arange(needed, dtype=jnp.int32)
    window = jnp.left_shift(jnp.int32(2), channel // group_width)
    position = jnp.arange(seq_rows, dtype=jnp.int32)[:, None]
    values = pool_in.astype(jnp.float32)
    summed = jnp.zeros_like(values)
    for offset in range(widest):
        shifted = jnp.pad(values, ((offset, 0), (0, 0)))[:seq_rows]
        summed = summed + jnp.where(offset < window, shifted, 0.0)
    counts = jnp.minimum(position + 1, window).astype(jnp.float32)
    pooled = (summed / counts - values).astype(jnp.bfloat16)
    map_bf = pool_map.astype(jnp.bfloat16)
    if local_channels < group_width:
        group_index = first_channel // group_width
        column_start = first_channel % group_width
        map_cols = lax.dynamic_slice(
            map_bf, (group_index, jnp.int32(0), column_start), (1, group_width, local_channels)
        )[0]
        grouped = jnp.dot(pooled, map_cols, preferred_element_type=jnp.float32)
    else:
        held_groups = local_channels // group_width
        maps_held = lax.dynamic_slice_in_dim(map_bf, first_channel // group_width, held_groups, 0)
        grouped = jnp.einsum(
            "tgc,gcd->tgd",
            pooled.reshape(seq_rows, held_groups, group_width),
            maps_held,
            preferred_element_type=jnp.float32,
        ).reshape(seq_rows, local_channels)
    pool_out = (grouped * pool_scale).astype(jnp.bfloat16)

    def mixer_rows(row_start, row_count):
        return jnp.dot(pool_out, out_full, preferred_element_type=jnp.float32)

    mixed = scatter_rows(mixer_rows, share)
    resid_two = resid_one + mixed * out_cols
    third = whole_rows(normed(resid_two, norm_gains[2]))
    ffn_two = ffn_partial(third, gate_full, up_full, down_full, hidden_scales, share)
    final_rows = (resid_two + 0.5 * (ffn_two * down_cols)).astype(jnp.bfloat16)
    return whole_rows(final_rows)


MESH = pl.DeviceIdType.MESH
PARTS = (1, 1, 4, 4)
FIRST_PART = (0, 1, 2, 6, 10)
TILE = 256
CHUNKS = 2
MIXER_AFTER = 1
bf16 = jnp.bfloat16
f32 = jnp.float32


def fits_kernel(mesh):
    return mesh.shape["rep"] == 2 and mesh.shape["fs"] == 4 and mesh.shape["tp"] == 4


def layer_kernel(
    n, tok, gains, gate_hbm, up_hbm, hs, down_hbm, mix_in_hbm, mix_out_hbm, isc, pmap, pool_scale, down_scale, out_scale,
    out, wide_gate, wide_up, wide_down, wide_in, wide_out, sc_in, gu_own, dn_own, gu_buf, dn_buf, wi_all, wo_all, sc_all, ps_all,
    ptok, first, gacc, hidden, stage, rs_a, s_z, rs_z, s_x, rs_x, r1, second, pool, r2, third, ra_2, sz_2, rz_2, sx_2, rx_2,
    z_send, y_send, w_recv, sc_send, sc_recv, tp_send, tp_recv, tk_send, tk_recv, rs_send, rs_recv, ag_send, ag_recv, loc,
):
    rep, fs, me = lax.axis_index("rep"), lax.axis_index("fs"), lax.axis_index("tp")
    seq, width = tok.shape
    slab = width // n
    share = seq // 4
    rows_half = seq // 2
    halo = widest
    window = rows_half + halo
    units = hs.shape[1]
    hu = units // 2
    groups, gc = pmap.shape[0], pmap.shape[1]
    core, chip = me % 2, me // 2
    mate = me + 1 - 2 * core
    across = (me + 2) % 4
    diag = (mate + 2) % 4
    peers = {1: mate, 2: across, 3: diag}
    partner = fs + 1 - 2 * (fs % 2)
    far_mid = jnp.where(fs < 2, 2, 1)
    far_end = jnp.where(fs < 2, 3, 0)
    order = (fs, partner, far_mid, far_end)
    middle = (fs == 1) | (fs == 2)
    kind = jnp.where(middle, 1, 0)
    kind_of = (kind, 1 - kind, 1, 0)

    def owner_cols(i):
        return pl.ds(pl.multiple_of(order[i] * slab, slab), slab)

    def cols_of(rank):
        return pl.ds(pl.multiple_of(rank * gc, gc), gc)

    half = slab // 2
    mine_half = pl.ds(pl.multiple_of(rep * half, half), half)
    other_half = pl.ds(pl.multiple_of((1 - rep) * half, half), half)
    loads = [
        pltpu.make_async_copy(mix_in_hbm.at[:, cols_of(me)], wide_in, loc.at[0]),
        pltpu.make_async_copy(mix_out_hbm, wide_out, loc.at[1]),
        pltpu.make_async_copy(gate_hbm.at[mine_half, :], wide_gate.at[mine_half, :], loc.at[2]),
        pltpu.make_async_copy(up_hbm.at[mine_half, :], wide_up.at[mine_half, :], loc.at[3]),
        pltpu.make_async_copy(gate_hbm.at[other_half, :], wide_gate.at[other_half, :], loc.at[4]),
        pltpu.make_async_copy(up_hbm.at[other_half, :], wide_up.at[other_half, :], loc.at[5]),
        pltpu.make_async_copy(down_hbm, wide_down, loc.at[6]),
    ]
    for load in loads:
        load.start()
    barrier = pltpu.get_barrier_semaphore()
    for i in (1, 2, 3):
        pl.semaphore_signal(barrier, inc=1, device_id={"fs": order[i]}, device_id_type=MESH)
    for k in (1, 2, 3):
        pl.semaphore_signal(barrier, inc=1, device_id={"tp": peers[k]}, device_id_type=MESH)
    pl.semaphore_signal(barrier, inc=1, device_id={"rep": 1 - rep}, device_id_type=MESH)

    sc_in[...] = jnp.zeros_like(sc_in)
    sc_in[0:1, :] = down_scale[...]
    sc_in[1:2, :] = out_scale[...]
    ps_all[me] = jnp.broadcast_to(pool_scale[...], ps_all.shape[1:])

    WI, WO, GU, DN = range(4)

    def piece(t, i, at, own_kind=None):
        shard = order[i]
        if t == WI:
            return wi_all.at[shard, pl.ds(pl.multiple_of(at * half, half), half), cols_of(me)]
        if t == WO:
            rows = gc // 2
            return wo_all.at[shard, pl.ds(pl.multiple_of(me * gc + at * rows, rows), rows), :]
        ref = (gu_own if t == GU else dn_own).at[own_kind] if own_kind is not None else (gu_buf if t == GU else dn_buf).at[shard]
        rows = ref.shape[0] // (2 * PARTS[t])
        return ref.at[pl.ds(pl.multiple_of(at * rows, rows), rows), :]

    started = []

    def start_if(cond, copy):
        if cond is None:
            copy.start()
        else:
            @pl.when(cond)
            def _():
                copy.start()
        started.append((cond, copy))

    def wait_sent():
        for cond, copy in started:
            if cond is None:
                copy.wait_send()
            else:
                @pl.when(cond)
                def _():
                    copy.wait_send()
        started.clear()

    def remote(src, dst, s_sem, r_sem, dev, cond=None):
        start_if(cond, pltpu.make_async_remote_copy(
            src_ref=src, dst_ref=dst, send_sem=s_sem, recv_sem=r_sem, device_id=dev, device_id_type=MESH
        ))

    def landed(dst, s_sem, r_sem):
        pltpu.make_async_remote_copy(
            src_ref=dst, dst_ref=dst, send_sem=s_sem, recv_sem=r_sem, device_id={"tp": mate}, device_id_type=MESH
        ).wait_recv()

    def send_own(t, i, u, cond=None):
        at = rep * PARTS[t] + u
        remote(
            piece(t, 0, at, kind_of[i] if t >= GU else None), piece(t, 0, at),
            z_send.at[i - 1, FIRST_PART[t] + u], w_recv.at[fs, 2 * FIRST_PART[t] + at], {"fs": order[i]}, cond,
        )

    def arrived(t, i, at):
        landed(piece(t, i, at), z_send.at[0, 0], w_recv.at[order[i], 2 * FIRST_PART[t] + at])

    def relay(t, i, u):
        at = rep * PARTS[t] + u
        arrived(t, i, at)
        here = piece(t, i, at)
        sem = w_recv.at[order[i], 2 * FIRST_PART[t] + at]
        if t < GU and i > 1:
            remote(here, here, y_send.at[0, i, FIRST_PART[t] + u], sem, {"fs": partner}, middle)
        remote(here, here, y_send.at[1, i, FIRST_PART[t] + u], sem, {"rep": 1 - rep})

    def rest(t, i):
        for u in range(PARTS[t]):
            arrived(t, i, (1 - rep) * PARTS[t] + u)

    loads[0].wait()
    loads[1].wait()
    wi_all[fs, :, cols_of(me)] = wide_in[...].astype(bf16)
    wo_all[fs, pl.ds(pl.multiple_of(me * gc, gc), gc), :] = wide_out[...].astype(bf16)

    def cast_gate_up(start, count, kinds):
        @pl.loop(0, count // 32)
        def _(j):
            rows = pl.ds(pl.multiple_of(start + j * 32, 32), 32)
            for h in kinds:
                cols = pl.ds(h * hu if isinstance(h, int) else pl.multiple_of(h * hu, 128), hu)
                gu_own[h, rows, 0:hu] = wide_gate[rows, cols].astype(bf16)
                gu_own[h, rows, hu:] = wide_up[rows, cols].astype(bf16)

    def my_rows(rank):
        return pl.ds(pl.multiple_of(rank * share, share), share)

    pl.semaphore_wait(barrier, n - 1 + 4)
    remote(tok.at[my_rows(me), :], ptok.at[my_rows(me), :], tk_send.at[0], tk_recv.at[0], {"fs": partner})
    loads[2].wait()
    loads[3].wait()
    for u in range(PARTS[GU]):
        cast_gate_up(rep * half + u * (half // PARTS[GU]), half // PARTS[GU], (0, 1))
        for i in (3, 2, 1):
            send_own(GU, i, u)
        if u == MIXER_AFTER:
            for t in (WI, WO):
                for i in (2, 1):
                    send_own(t, i, 0)

    def spread(t, i, rank):
        return wi_all.at[order[i], :, cols_of(rank)] if t == WI else wo_all.at[order[i], pl.ds(pl.multiple_of(rank * gc, gc), gc), :]

    def share_mixer(i):
        for t in (WI, WO):
            mine = spread(t, i, me)
            remote(mine, mine, tp_send.at[t, i, 1], tp_recv.at[t, i, 1], {"tp": across})
            remote(mine, mine, tp_send.at[t, i, 0], tp_recv.at[t, i, 0], {"tp": mate})

    def pass_mixer(i):
        for t in (WI, WO):
            theirs = spread(t, i, across)
            landed(theirs, tp_send.at[t, i, 1], tp_recv.at[t, i, 1])
            remote(theirs, theirs, tp_send.at[t, i, 2], tp_recv.at[t, i, 2], {"tp": mate})

    def have_mixer(i):
        for t in (WI, WO):
            landed(spread(t, i, mate), tp_send.at[t, i, 0], tp_recv.at[t, i, 0])
            landed(spread(t, i, diag), tp_send.at[t, i, 2], tp_recv.at[t, i, 2])

    share_mixer(0)
    loads[4].wait()
    loads[5].wait()
    cast_gate_up((1 - rep) * half, half, (kind,))
    loads[6].wait()

    @pl.loop(0, hu // 32)
    def _(j):
        rows = pl.ds(pl.multiple_of(j * 32, 32), 32)
        for h in (0, 1):
            dn_own[h, rows, :] = wide_down[pl.ds(pl.multiple_of(h * hu + j * 32, 32), 32), :].astype(bf16)

    for i in (1, 2, 3):
        remote(sc_in, sc_all.at[fs], sc_send.at[i - 1], sc_recv.at[fs], {"fs": order[i]})
    for k in (1, 2, 3):
        remote(ps_all.at[me], ps_all.at[me], tp_send.at[2, 0, k - 1], tp_recv.at[2, 0, k - 1], {"tp": peers[k]})

    def normed_rows(values, gain):
        mean_sq = jnp.mean(values * values, axis=-1, keepdims=True)
        return (values * lax.rsqrt(mean_sq + eps) * gain).astype(bf16)

    stage[:, :, 0:halo, :] = jnp.zeros((n, 2, halo, slab), bf16)

    def norm_first(source, top):
        @pl.loop(0, seq // 32)
        def _(j):
            rows = pl.ds(pl.multiple_of(j * 32, 32), 32)
            first[pl.ds(pl.multiple_of(top + j * 32, 32), 32), :] = normed_rows(source[rows, :].astype(f32), gains[0:1, :])

    def dot(a, b):
        return jnp.dot(a, b, preferred_element_type=f32)

    def held_gu(i):
        return gu_own.at[kind] if i == 0 else gu_buf.at[order[i]]

    def held_dn(i):
        return dn_own.at[kind] if i == 0 else dn_buf.at[order[i]]

    def gate_up(i, fresh):
        weights = held_gu(i)
        cols = owner_cols(i)

        @pl.loop(0, 2 * hu // TILE)
        def _(j):
            at = pl.ds(pl.multiple_of(j * TILE, TILE), TILE)
            term = dot(first[:, cols], weights[:, at])
            if fresh:
                gacc[:, at] = term
            else:
                gacc[:, at] += term

    def activate(rows):
        @pl.loop(0, hu // 128)
        def _(j):
            at = pl.ds(pl.multiple_of(j * 128, 128), 128)
            up_at = pl.ds(pl.multiple_of(hu + j * 128, 128), 128)
            sc_at = pl.ds(pl.multiple_of(kind * hu + j * 128, 128), 128)
            gate = gacc[rows, at] * hs[0:1, sc_at]
            upper = gacc[rows, up_at] * hs[1:2, sc_at]
            hidden[rows, at] = (gate / (1.0 + jnp.exp(-gate)) * upper).astype(bf16)

    def down(i, side, top):
        weights = held_dn(i)

        @pl.loop(0, slab // TILE)
        def _(j):
            at = pl.ds(pl.multiple_of(j * TILE, TILE), TILE)
            stage[i, side, top:top + seq, at] = dot(hidden[side * seq:(side + 1) * seq, :], weights[:, at]).astype(bf16)

    norm_first(tok, 0)
    own_rows = my_rows(me)
    landed(ptok.at[own_rows, :], tk_send.at[0], tk_recv.at[0])
    for k in (2, 3, 1):
        remote(ptok.at[own_rows, :], ptok.at[own_rows, :], tk_send.at[k], tk_recv.at[k], {"tp": peers[k]})
    def relay_mixer(i):
        for t in (WI, WO):
            relay(t, i, 0)

    def rest_mixer(i):
        rest(WI, i)
        rest(WO, i)
        share_mixer(i)

    for u in range(PARTS[GU]):
        for i in (1, 2, 3):
            relay(GU, i, u)
        if u == 1:
            for k in (1, 2, 3):
                landed(ptok.at[my_rows(peers[k]), :], tk_send.at[k], tk_recv.at[k])
            norm_first(ptok, seq)
        if u == 2:
            relay_mixer(1)
            for i in (1, 2, 3):
                for v in range(PARTS[DN]):
                    send_own(DN, i, v, middle if i == 3 else None)
            gate_up(0, True)
    relay_mixer(2)
    relay_mixer(3)
    rest_mixer(1)
    rest(GU, 1)
    gate_up(1, False)
    pass_mixer(0)
    rest(GU, 2)
    gate_up(2, False)
    rest_mixer(2)
    rest_mixer(3)
    rest(GU, 3)
    gate_up(3, False)
    activate(slice(None))

    for i in (1, 2, 3):
        landed(sc_all.at[order[i]], sc_send.at[0], sc_recv.at[order[i]])

    def scales(i):
        return sc_in if i == 0 else sc_all.at[order[i]]

    def window_of(c):
        return pl.ds(pl.multiple_of(c * rows_half, rows_half), window)

    def half_of(c):
        return pl.ds(pl.multiple_of(c * rows_half, rows_half), rows_half)

    before = pl.ds(pl.multiple_of((core * rows_half + seq - halo) % seq, halo), halo)

    def cut_one(i, part, top, picked, got, sems):
        for side in (1, 0):
            down(i, side, top)
            remote(stage.at[i, side, picked(1 - core), :], got.at[i, side], rs_send.at[sems, i, side], rs_recv.at[sems, i, side], {"tp": mate})

    def cross_one(i, picked, got, sent, there, sems):
        landed(got.at[i, 1], rs_send.at[sems, i, 1], rs_recv.at[sems, i, 1])
        sent[i] = (stage[i, 1, picked(core), :].astype(f32) + got[i, 1].astype(f32)).astype(bf16)
        remote(sent.at[i], there.at[fs_slab(i)], rs_send.at[sems, i, 2], rz_recv(sems, i), {"fs": partner})

    def fs_slab(i):
        return order[i]

    def rz_recv(sems, i):
        return rs_recv.at[sems, order[i], 2]

    def fold_one(i, picked, got, there, sent, far, sems):
        landed(got.at[i, 0], rs_send.at[sems, i, 0], rs_recv.at[sems, i, 0])
        landed(there.at[fs_slab(i)], rs_send.at[sems, i, 2], rz_recv(sems, i))
        total = stage[i, 0, picked(core), :].astype(f32) + got[i, 0].astype(f32) + there[fs_slab(i)].astype(f32)
        sent[i] = total.astype(bf16)
        remote(sent.at[i], far.at[i], rs_send.at[sems, i, 3], rs_recv.at[sems, i, 3], {"tp": across})

    def total_of(i, sent, far, sems):
        landed(far.at[i], rs_send.at[sems, i, 3], rs_recv.at[sems, i, 3])
        return 0.5 * ((sent[i].astype(f32) + far[i].astype(f32)) * scales(i)[0:1, :])

    def cut_a(i):
        cut_one(i, None, halo, window_of, rs_a, 0)

    def cross_a(i):
        cross_one(i, window_of, rs_a, s_z, rs_z, 0)

    def fold_a(i):
        fold_one(i, window_of, rs_a, rs_z, s_x, rs_x, 0)

    def gather_a(i):
        total = total_of(i, s_x, rs_x, 0)
        cols = owner_cols(i)
        r1[0:halo, cols] = total[0:halo] + jnp.where(core > 0, tok[before, cols].astype(f32), 0.0)
        r1[halo:, cols] = total[halo:] + tok[half_of(core), cols].astype(f32)

    cut_a(0)
    for u in range(PARTS[DN]):
        relay(DN, 1, u)
    cross_a(0)
    for u in range(PARTS[DN]):
        send_own(DN, 3, u, ~middle)
    for u in range(PARTS[DN]):
        relay(DN, 2, u)
    pass_mixer(1)
    rest(DN, 1)
    cut_a(1)
    cross_a(1)
    fold_a(0)
    for u in range(PARTS[DN]):
        relay(DN, 3, u)
    rest(DN, 2)
    cut_a(2)
    pass_mixer(2)
    cross_a(2)
    fold_a(1)
    rest(DN, 3)
    cut_a(3)
    pass_mixer(3)
    cross_a(3)
    gather_a(0)
    fold_a(2)
    gather_a(1)
    for k in (1, 2, 3):
        landed(ps_all.at[peers[k]], tp_send.at[2, 0, k - 1], tp_recv.at[2, 0, k - 1])
    for i in range(n):
        have_mixer(i)
    fold_a(3)
    gather_a(2)
    gather_a(3)

    second[...] = normed_rows(r1[...], gains[1:2, :])
    total = dot(second[:, owner_cols(0)], wi_all[order[0]])
    for i in range(1, n):
        total = total + dot(second[:, owner_cols(i)], wi_all[order[i]])
    values = (total * isc[...]).astype(bf16).astype(f32)
    sums = values
    position = lax.broadcasted_iota(jnp.int32, (rows_half, gc), 0) + core * rows_half
    for g in range(groups):
        span = 2 ** (g + 1)
        sums = sums + pltpu.roll(sums, span // 2, 0)
        at = slice(g * gc, (g + 1) * gc)
        counts = jnp.minimum(position + 1, span).astype(f32)
        pooled = (sums[halo:, 0:gc] / counts - values[halo:, at]).astype(bf16)
        pool[:, at] = (dot(pooled, pmap[g].astype(bf16)) * ps_all[g, 0:1, :]).astype(bf16)
        sums = sums[:, gc:]
    for i in range(n):
        cols = owner_cols(i)
        r2[:, cols] = r1[halo:, cols] + dot(pool[...], wo_all[order[i]]) * scales(i)[1:2, :]
    third[half_of(core), :] = normed_rows(r2[...], gains[2:3, :])
    wait_sent()

    def quarter(c, x):
        return pl.ds(pl.multiple_of(c * rows_half + x * share, share), share)

    def beside(c, x):
        return pl.ds(pl.multiple_of(seq + c * rows_half + x * share, share), share)

    span_cols = width // CHUNKS
    chunk = [slice(j * span_cols, (j + 1) * span_cols) for j in range(CHUNKS)]
    for j in range(CHUNKS):
        remote(third.at[quarter(core, chip), chunk[j]], third.at[beside(core, chip), chunk[j]], ag_send.at[j, 1], ag_recv.at[j, 1], {"fs": partner})
    mine = third.at[half_of(core), :]
    remote(mine, mine, ag_send.at[0, 0], ag_recv.at[0, 0], {"tp": mate})

    def hidden_rows(side):
        rows = slice(side * seq, (side + 1) * seq)

        @pl.loop(0, 2 * hu // TILE)
        def _(j):
            at = pl.ds(pl.multiple_of(j * TILE, TILE), TILE)
            acc = dot(third[rows, owner_cols(0)], held_gu(0)[:, at])
            for i in range(1, n):
                acc = acc + dot(third[rows, owner_cols(i)], held_gu(i)[:, at])
            gacc[rows, at] = acc

        activate(rows)

    def forward_third(j):
        here = third.at[beside(core, chip), chunk[j]]
        landed(here, ag_send.at[j, 1], ag_recv.at[j, 1])
        remote(here, here, ag_send.at[j, 2], ag_recv.at[j, 2], {"tp": across})
        remote(here, here, ag_send.at[j, 3], ag_recv.at[j, 3], {"tp": mate})

    def pass_third(j):
        there = third.at[beside(core, 1 - chip), chunk[j]]
        landed(there, ag_send.at[j, 2], ag_recv.at[j, 2])
        remote(there, there, ag_send.at[j, 4], ag_recv.at[j, 4], {"tp": mate})

    landed(third.at[half_of(1 - core), :], ag_send.at[0, 0], ag_recv.at[0, 0])
    hidden_rows(0)
    forward_third(0)
    for i in range(n):
        down(i, 0, 0)
        remote(stage.at[i, 0, half_of(1 - core), :], ra_2.at[i, 0], rs_send.at[1, i, 0], rs_recv.at[1, i, 0], {"tp": mate})
        if i + 1 < CHUNKS:
            forward_third(i + 1)
    for j in range(CHUNKS):
        pass_third(j)
    for j in range(CHUNKS):
        landed(third.at[beside(1 - core, chip), chunk[j]], ag_send.at[j, 3], ag_recv.at[j, 3])
        landed(third.at[beside(1 - core, 1 - chip), chunk[j]], ag_send.at[j, 4], ag_recv.at[j, 4])
    hidden_rows(1)

    def cross_b(i):
        cross_one(i, half_of, ra_2, sz_2, rz_2, 1)

    def fold_b(i):
        fold_one(i, half_of, ra_2, rz_2, sx_2, rx_2, 1)

    def final_b(i):
        total = total_of(i, sx_2, rx_2, 1)
        cols = owner_cols(i)
        out[half_of(core), cols] = (r2[:, cols] + total).astype(bf16)
        done = out.at[half_of(core), cols]
        remote(done, done, ag_send.at[i, 5], ag_recv.at[i, 5], {"tp": mate})

    for i in range(n):
        down(i, 1, 0)
        remote(stage.at[i, 1, half_of(1 - core), :], ra_2.at[i, 1], rs_send.at[1, i, 1], rs_recv.at[1, i, 1], {"tp": mate})
        if i > 0:
            cross_b(i - 1)
    cross_b(n - 1)
    for i in range(n):
        fold_b(i)
        if i > 0:
            final_b(i - 1)
    final_b(n - 1)
    for i in range(n):
        landed(out.at[half_of(1 - core), owner_cols(i)], ag_send.at[i, 5], ag_recv.at[i, 5])
    wait_sent()


def fused_layer(
    tokens, norm_gains, gate_weight, up_weight, hidden_scales, down_weight, down_scale, mix_in, in_scale,
    pool_map, pool_scale, mix_out, out_scale,
):
    n = lax.axis_size("fs")
    seq, width = tokens.shape
    slab, units = gate_weight.shape
    hu = units // 2
    groups, gc, _ = pool_map.shape
    rows_half = seq // 2
    window = rows_half + widest
    vmem = pl.BlockSpec(memory_space=pltpu.VMEM)
    dma = pltpu.SemaphoreType.DMA
    hbm = pl.BlockSpec(memory_space=pl.ANY)
    args = (
        (tokens, vmem), (norm_gains, vmem), (gate_weight, hbm), (up_weight, hbm), (hidden_scales, vmem),
        (down_weight, hbm), (mix_in, hbm), (mix_out, hbm), (in_scale[None], vmem), (pool_map, vmem),
        (pool_scale[None], vmem), (down_scale[None], vmem), (out_scale[None], vmem),
    )
    return pl.pallas_call(
        functools.partial(layer_kernel, n),
        out_shape=jax.ShapeDtypeStruct((seq, width), bf16),
        in_specs=[spec for _, spec in args],
        out_specs=vmem,
        scratch_shapes=[
            pltpu.VMEM((slab, units), f32),
            pltpu.VMEM((slab, units), f32),
            pltpu.VMEM((units, slab), f32),
            pltpu.VMEM((slab, gc), f32),
            pltpu.VMEM((gc, slab), f32),
            pltpu.VMEM((8, slab), f32),
            pltpu.VMEM((2, slab, 2 * hu), bf16),
            pltpu.VMEM((2, hu, slab), bf16),
            pltpu.VMEM((n, slab, 2 * hu), bf16),
            pltpu.VMEM((n, hu, slab), bf16),
            pltpu.VMEM((n, slab, groups * gc), bf16),
            pltpu.VMEM((n, groups * gc, slab), bf16),
            pltpu.VMEM((n, 8, slab), f32),
            pltpu.VMEM((4, 8, gc), f32),
            pltpu.VMEM((seq, width), bf16),
            pltpu.VMEM((2 * seq, width), bf16),
            pltpu.VMEM((2 * seq, 2 * hu), f32),
            pltpu.VMEM((2 * seq, hu), bf16),
            pltpu.VMEM((n, 2, seq + widest, slab), bf16),
            pltpu.VMEM((n, 2, window, slab), bf16),
            pltpu.VMEM((n, window, slab), bf16),
            pltpu.VMEM((n, window, slab), bf16),
            pltpu.VMEM((n, window, slab), bf16),
            pltpu.VMEM((n, window, slab), bf16),
            pltpu.VMEM((window, width), f32),
            pltpu.VMEM((window, width), bf16),
            pltpu.VMEM((rows_half, groups * gc), bf16),
            pltpu.VMEM((rows_half, width), f32),
            pltpu.VMEM((2 * seq, width), bf16),
            pltpu.VMEM((n, 2, rows_half, slab), bf16),
            pltpu.VMEM((n, rows_half, slab), bf16),
            pltpu.VMEM((n, rows_half, slab), bf16),
            pltpu.VMEM((n, rows_half, slab), bf16),
            pltpu.VMEM((n, rows_half, slab), bf16),
            dma((n - 1, FIRST_PART[-1])), dma((2, n, FIRST_PART[-1])), dma((n, 2 * FIRST_PART[-1])),
            dma((n - 1,)), dma((n,)),
            dma((3, n, 3)), dma((3, n, 3)),
            dma((4,)), dma((4,)),
            dma((2, n, 4)), dma((2, n, 4)),
            dma((n, 6)), dma((n, 6)),
            dma((7,)),
        ],
        compiler_params=pltpu.CompilerParams(
            collective_id=0, has_side_effects=True, vmem_limit_bytes=60 * 1024 * 1024
        ),
    )(*[value for value, _ in args])


def solution(mesh):
    body = fused_layer if fits_kernel(mesh) else per_device
    return jax.shard_map(
        body,
        mesh=mesh,
        in_specs=(
            P(("rep", "fs"), None),
            P(),
            P("fs", "tp"),
            P("fs", "tp"),
            P(None, "tp"),
            P("tp", "fs"),
            P("fs"),
            P("fs", None),
            P(),
            P(),
            P("tp"),
            P("tp", "fs"),
            P("fs"),
        ),
        out_specs=P(("rep", "fs"), None),
        check_vma=False,
    )
```

time: 151 us -> 140 us (0.927)
  Pallas kernels: 148 us -> 136 us
    pallas_call x1, Pallas kernels: 148 us -> 136 us  [fused_layer(): pl.pallas_call(functools.partial(layer_kernel, n), out_shape=jax.ShapeDty...]
where the time goes in v1:
time: 140 us; the launch traced here: 139 us
  Pallas kernels  136 us (97%)
  local copies, waits for them, and re-layouts  2.3 us (2%)
    pallas_call x1, Pallas kernels, fused_layer(): pl.pallas_call(functools.partial(layer_kernel, n), out_shape=jax.ShapeDty...  136 us

profile of v1, /device:TPU:1, one launch (start us, length us, event | category | flops | bytes accessed | tf_op | source)
XLA Modules:
  0.0 138.8 jit_solution(16106864951683379039)
XLA Ops:
  0.0 136.5 %shard_map.127 = bf16[256,2048]{1,0:T(8,128)(2,1)} custom-call(bf16[256,2048]{1,0:T(8,128)(2,1)} %tok.1, f32[3,2048]{1,0:T(4,128)} %gains.1, f32[512,768]{1,0:T(8,128)} %gate_hbm.1, f32[512,768]{1,0:T(8,128)} %up_hbm.1, f32[2,768]{1,0:T(2,128)} %hs.1, f32[768,512]{1,0:T(8,128)} %down_hbm.1, f32[512,512]{1,0:T(8,128)} %mix_in_hbm.1, f32[128,512]{1,0:T(8,128)} %mix_out_hbm.1, ...), custom_call_target="tpu_custom_call" | custom-call | tf_op jit(solution)/shard_map/pallas_call | solution.py:656
  136.5 2.3 %copy.15 = bf16[256,2048]{1,0:T(8,128)(2,1)} copy(bf16[256,2048]{1,0:T(8,128)(2,1)} %shard_map.127) | data formatting | bytes 2097152

commit v2 on v1

--- a/solution.py
+++ b/solution.py
@@ -143,7 +143,7 @@
 PARTS = (1, 1, 4, 4)
 FIRST_PART = (0, 1, 2, 6, 10)
 TILE = 256
-CHUNKS = 2
+BATCHES = 2
 MIXER_AFTER = 1
 bf16 = jnp.bfloat16
 f32 = jnp.float32
@@ -156,8 +156,8 @@
 def layer_kernel(
     n, tok, gains, gate_hbm, up_hbm, hs, down_hbm, mix_in_hbm, mix_out_hbm, isc, pmap, pool_scale, down_scale, out_scale,
     out, wide_gate, wide_up, wide_down, wide_in, wide_out, sc_in, gu_own, dn_own, gu_buf, dn_buf, wi_all, wo_all, sc_all, ps_all,
-    ptok, first, gacc, hidden, stage, rs_a, s_z, rs_z, s_x, rs_x, r1, second, pool, r2, third, ra_2, sz_2, rz_2, sx_2, rx_2,
-    z_send, y_send, w_recv, sc_send, sc_recv, tp_send, tp_recv, tk_send, tk_recv, rs_send, rs_recv, ag_send, ag_recv, loc,
+    ptok, first, gacc, hidden, stage, rs_a, s_z, rs_z, s_x, rs_x, r1, second, pool, r2, third, stage_2, ra_2, sz_2, rz_2, sx_2, rx_2,
+    z_send, y_send, w_recv, sc_send, sc_recv, tp_send, tp_recv, tk_send, tk_recv, rs_send, rs_recv, rt_send, rt_recv, ag_send, ag_recv, loc,
 ):
     rep, fs, me = lax.axis_index("rep"), lax.axis_index("fs"), lax.axis_index("tp")
     seq, width = tok.shape
@@ -392,13 +392,13 @@
             upper = gacc[rows, up_at] * hs[1:2, sc_at]
             hidden[rows, at] = (gate / (1.0 + jnp.exp(-gate)) * upper).astype(bf16)
 
-    def down(i, side, top):
+    def down(i, side):
         weights = held_dn(i)
 
         @pl.loop(0, slab // TILE)
         def _(j):
             at = pl.ds(pl.multiple_of(j * TILE, TILE), TILE)
-            stage[i, side, top:top + seq, at] = dot(hidden[side * seq:(side + 1) * seq, :], weights[:, at]).astype(bf16)
+            stage[i, side, halo:, at] = dot(hidden[side * seq:(side + 1) * seq, :], weights[:, at]).astype(bf16)
 
     norm_first(tok, 0)
     own_rows = my_rows(me)
@@ -447,55 +447,59 @@
     def scales(i):
         return sc_in if i == 0 else sc_all.at[order[i]]
 
-    def window_of(c):
-        return pl.ds(pl.multiple_of(c * rows_half, rows_half), window)
-
     def half_of(c):
         return pl.ds(pl.multiple_of(c * rows_half, rows_half), rows_half)
 
     before = pl.ds(pl.multiple_of((core * rows_half + seq - halo) % seq, halo), halo)
-
-    def cut_one(i, part, top, picked, got, sems):
+    batch = rows_half // BATCHES
+    whole = ((0, window),)
+    split = tuple((b * batch + (halo if b else 0), batch + (0 if b else halo)) for b in range(BATCHES))
+
+    def parts(i):
+        return split if i == n - 1 else whole
+
+    def window_of(c, part):
+        return pl.ds(pl.multiple_of(c * rows_half + part[0], halo), part[1])
+
+    def cut_a(i):
         for side in (1, 0):
-            down(i, side, top)
-            remote(stage.at[i, side, picked(1 - core), :], got.at[i, side], rs_send.at[sems, i, side], rs_recv.at[sems, i, side], {"tp": mate})
-
-    def cross_one(i, picked, got, sent, there, sems):
-        landed(got.at[i, 1], rs_send.at[sems, i, 1], rs_recv.at[sems, i, 1])
-        sent[i] = (stage[i, 1, picked(core), :].astype(f32) + got[i, 1].astype(f32)).astype(bf16)
-        remote(sent.at[i], there.at[fs_slab(i)], rs_send.at[sems, i, 2], rz_recv(sems, i), {"fs": partner})
-
-    def fs_slab(i):
-        return order[i]
-
-    def rz_recv(sems, i):
-        return rs_recv.at[sems, order[i], 2]
-
-    def fold_one(i, picked, got, there, sent, far, sems):
-        landed(got.at[i, 0], rs_send.at[sems, i, 0], rs_recv.at[sems, i, 0])
-        landed(there.at[fs_slab(i)], rs_send.at[sems, i, 2], rz_recv(sems, i))
-        total = stage[i, 0, picked(core), :].astype(f32) + got[i, 0].astype(f32) + there[fs_slab(i)].astype(f32)
-        sent[i] = total.astype(bf16)
-        remote(sent.at[i], far.at[i], rs_send.at[sems, i, 3], rs_recv.at[sems, i, 3], {"tp": across})
-
-    def total_of(i, sent, far, sems):
-        landed(far.at[i], rs_send.at[sems, i, 3], rs_recv.at[sems, i, 3])
-        return 0.5 * ((sent[i].astype(f32) + far[i].astype(f32)) * scales(i)[0:1, :])
-
-    def cut_a(i):
-        cut_one(i, None, halo, window_of, rs_a, 0)
+            down(i, side)
+            for p, part in enumerate(parts(i)):
+                remote(
+                    stage.at[i, side, window_of(1 - core, part), :], rs_a.at[i, side, pl.ds(*part), :],
+                    rs_send.at[p, i, side], rs_recv.at[p, i, side], {"tp": mate},
+                )
 
     def cross_a(i):
-        cross_one(i, window_of, rs_a, s_z, rs_z, 0)
-
-    def fold_a(i):
-        fold_one(i, window_of, rs_a, rs_z, s_x, rs_x, 0)
-
-    def gather_a(i):
-        total = total_of(i, s_x, rs_x, 0)
+        for p, part in enumerate(parts(i)):
+            rows = pl.ds(*part)
+            landed(rs_a.at[i, 1, rows, :], rs_send.at[p, i, 1], rs_recv.at[p, i, 1])
+            s_z[i, rows, :] = (stage[i, 1, window_of(core, part), :].astype(f32) + rs_a[i, 1, rows, :].astype(f32)).astype(bf16)
+            remote(
+                s_z.at[i, rows, :], rs_z.at[order[i], rows, :], rs_send.at[p, i, 2], rs_recv.at[p, order[i], 2], {"fs": partner}
+            )
+
+    def fold_a(i, p=0):
+        part = parts(i)[p]
+        rows = pl.ds(*part)
+        landed(rs_a.at[i, 0, rows, :], rs_send.at[p, i, 0], rs_recv.at[p, i, 0])
+        landed(rs_z.at[order[i], rows, :], rs_send.at[p, i, 2], rs_recv.at[p, order[i], 2])
+        total = stage[i, 0, window_of(core, part), :].astype(f32) + rs_a[i, 0, rows, :].astype(f32)
+        s_x[i, rows, :] = (total + rs_z[order[i], rows, :].astype(f32)).astype(bf16)
+        remote(s_x.at[i, rows, :], rs_x.at[i, rows, :], rs_send.at[p, i, 3], rs_recv.at[p, i, 3], {"tp": across})
+
+    def gather_a(i, p=0):
+        part = parts(i)[p]
+        top, count = part
+        rows = pl.ds(*part)
+        landed(rs_x.at[i, rows, :], rs_send.at[p, i, 3], rs_recv.at[p, i, 3])
+        total = 0.5 * ((s_x[i, rows, :].astype(f32) + rs_x[i, rows, :].astype(f32)) * scales(i)[0:1, :])
         cols = owner_cols(i)
-        r1[0:halo, cols] = total[0:halo] + jnp.where(core > 0, tok[before, cols].astype(f32), 0.0)
-        r1[halo:, cols] = total[halo:] + tok[half_of(core), cols].astype(f32)
+        if top == 0:
+            r1[0:halo, cols] = total[0:halo] + jnp.where(core > 0, tok[before, cols].astype(f32), 0.0)
+            total, top, count = total[halo:], halo, count - halo
+        held = pl.ds(pl.multiple_of(core * rows_half + top - halo, halo), count)
+        r1[top:top + count, cols] = total + tok[held, cols].astype(f32)
 
     cut_a(0)
     for u in range(PARTS[DN]):
@@ -528,46 +532,66 @@
         landed(ps_all.at[peers[k]], tp_send.at[2, 0, k - 1], tp_recv.at[2, 0, k - 1])
     for i in range(n):
         have_mixer(i)
-    fold_a(3)
     gather_a(2)
-    gather_a(3)
-
-    second[...] = normed_rows(r1[...], gains[1:2, :])
-    total = dot(second[:, owner_cols(0)], wi_all[order[0]])
-    for i in range(1, n):
-        total = total + dot(second[:, owner_cols(i)], wi_all[order[i]])
-    values = (total * isc[...]).astype(bf16).astype(f32)
-    sums = values
-    position = lax.broadcasted_iota(jnp.int32, (rows_half, gc), 0) + core * rows_half
-    for g in range(groups):
-        span = 2 ** (g + 1)
-        sums = sums + pltpu.roll(sums, span // 2, 0)
-        at = slice(g * gc, (g + 1) * gc)
-        counts = jnp.minimum(position + 1, span).astype(f32)
-        pooled = (sums[halo:, 0:gc] / counts - values[halo:, at]).astype(bf16)
-        pool[:, at] = (dot(pooled, pmap[g].astype(bf16)) * ps_all[g, 0:1, :]).astype(bf16)
-        sums = sums[:, gc:]
-    for i in range(n):
-        cols = owner_cols(i)
-        r2[:, cols] = r1[halo:, cols] + dot(pool[...], wo_all[order[i]]) * scales(i)[1:2, :]
-    third[half_of(core), :] = normed_rows(r2[...], gains[2:3, :])
-    wait_sent()
-
-    def quarter(c, x):
-        return pl.ds(pl.multiple_of(c * rows_half + x * share, share), share)
-
-    def beside(c, x):
-        return pl.ds(pl.multiple_of(seq + c * rows_half + x * share, share), share)
-
-    span_cols = width // CHUNKS
-    chunk = [slice(j * span_cols, (j + 1) * span_cols) for j in range(CHUNKS)]
-    for j in range(CHUNKS):
-        remote(third.at[quarter(core, chip), chunk[j]], third.at[beside(core, chip), chunk[j]], ag_send.at[j, 1], ag_recv.at[j, 1], {"fs": partner})
-    mine = third.at[half_of(core), :]
-    remote(mine, mine, ag_send.at[0, 0], ag_recv.at[0, 0], {"tp": mate})
-
-    def hidden_rows(side):
-        rows = slice(side * seq, (side + 1) * seq)
+
+    def mixer(b):
+        low = b * batch
+        taken = slice(low, low + batch + halo)
+        second[...] = normed_rows(r1[taken, :], gains[1:2, :])
+        total = dot(second[:, owner_cols(0)], wi_all[order[0]])
+        for i in range(1, n):
+            total = total + dot(second[:, owner_cols(i)], wi_all[order[i]])
+        values = (total * isc[...]).astype(bf16).astype(f32)
+        sums = values
+        position = lax.broadcasted_iota(jnp.int32, (batch, gc), 0) + (core * rows_half + low)
+        for g in range(groups):
+            span = 2 ** (g + 1)
+            sums = sums + pltpu.roll(sums, span // 2, 0)
+            at = slice(g * gc, (g + 1) * gc)
+            counts = jnp.minimum(position + 1, span).astype(f32)
+            pooled = (sums[halo:, 0:gc] / counts - values[halo:, at]).astype(bf16)
+            pool[:, at] = (dot(pooled, pmap[g].astype(bf16)) * ps_all[g, 0:1, :]).astype(bf16)
+            sums = sums[:, gc:]
+        rows = slice(low, low + batch)
+        for i in range(n):
+            cols = owner_cols(i)
+            r2[rows, cols] = r1[low + halo:low + halo + batch, cols] + dot(pool[...], wo_all[order[i]]) * scales(i)[1:2, :]
+        third[lot(b, 0, core), :] = normed_rows(r2[rows, :], gains[2:3, :])
+
+    def lot(b, side, c):
+        return pl.ds(pl.multiple_of(((b * 2 + side) * 2 + c) * batch, batch), batch)
+
+    def piece_of(b, side, c, x):
+        return pl.ds(pl.multiple_of(((b * 2 + side) * 2 + c) * batch + x * (batch // 2), batch // 2), batch // 2)
+
+    def both(b, side):
+        return slice((b * 2 + side) * 2 * batch, (b * 2 + side + 1) * 2 * batch)
+
+    def send_third(b):
+        remote(third.at[piece_of(b, 0, core, chip), :], third.at[piece_of(b, 1, core, chip), :], ag_send.at[b, 1], ag_recv.at[b, 1], {"fs": partner})
+        mine = third.at[lot(b, 0, core), :]
+        remote(mine, mine, ag_send.at[b, 0], ag_recv.at[b, 0], {"tp": mate})
+
+    def have_own(b):
+        landed(third.at[lot(b, 0, 1 - core), :], ag_send.at[b, 0], ag_recv.at[b, 0])
+
+    def forward_third(b):
+        here = third.at[piece_of(b, 1, core, chip), :]
+        landed(here, ag_send.at[b, 1], ag_recv.at[b, 1])
+        remote(here, here, ag_send.at[b, 2], ag_recv.at[b, 2], {"tp": across})
+        remote(here, here, ag_send.at[b, 3], ag_recv.at[b, 3], {"tp": mate})
+
+    def pass_third(b):
+        there = third.at[piece_of(b, 1, core, 1 - chip), :]
+        landed(there, ag_send.at[b, 2], ag_recv.at[b, 2])
+        remote(there, there, ag_send.at[b, 4], ag_recv.at[b, 4], {"tp": mate})
+
+    def have_partner(b):
+        landed(third.at[piece_of(b, 1, 1 - core, chip), :], ag_send.at[b, 3], ag_recv.at[b, 3])
+        landed(third.at[piece_of(b, 1, 1 - core, 1 - chip), :], ag_send.at[b, 4], ag_recv.at[b, 4])
+
+    def hidden_rows(b, side):
+        rows = both(b, side)
 
         @pl.loop(0, 2 * hu // TILE)
         def _(j):
@@ -579,58 +603,78 @@
 
         activate(rows)
 
-    def forward_third(j):
-        here = third.at[beside(core, chip), chunk[j]]
-        landed(here, ag_send.at[j, 1], ag_recv.at[j, 1])
-        remote(here, here, ag_send.at[j, 2], ag_recv.at[j, 2], {"tp": across})
-        remote(here, here, ag_send.at[j, 3], ag_recv.at[j, 3], {"tp": mate})
-
-    def pass_third(j):
-        there = third.at[beside(core, 1 - chip), chunk[j]]
-        landed(there, ag_send.at[j, 2], ag_recv.at[j, 2])
-        remote(there, there, ag_send.at[j, 4], ag_recv.at[j, 4], {"tp": mate})
-
-    landed(third.at[half_of(1 - core), :], ag_send.at[0, 0], ag_recv.at[0, 0])
-    hidden_rows(0)
+    def down_send(i, b, side):
+        rows = both(b, side)
+        stage_2[i, rows, :] = dot(hidden[rows, :], held_dn(i)[...]).astype(bf16)
+        remote(stage_2.at[i, lot(b, side, 1 - core), :], ra_2.at[i, b, side], rt_send.at[i, b, side], rt_recv.at[i, b, side], {"tp": mate})
+
+    def cross_b(i, b):
+        landed(ra_2.at[i, b, 1], rt_send.at[i, b, 1], rt_recv.at[i, b, 1])
+        sz_2[i, b] = (stage_2[i, lot(b, 1, core), :].astype(f32) + ra_2[i, b, 1].astype(f32)).astype(bf16)
+        remote(sz_2.at[i, b], rz_2.at[order[i], b], rt_send.at[i, b, 2], rt_recv.at[order[i], b, 2], {"fs": partner})
+
+    def fold_b(i, b):
+        landed(ra_2.at[i, b, 0], rt_send.at[i, b, 0], rt_recv.at[i, b, 0])
+        landed(rz_2.at[order[i], b], rt_send.at[i, b, 2], rt_recv.at[order[i], b, 2])
+        total = stage_2[i, lot(b, 0, core), :].astype(f32) + ra_2[i, b, 0].astype(f32) + rz_2[order[i], b].astype(f32)
+        sx_2[i, b] = total.astype(bf16)
+        remote(sx_2.at[i, b], rx_2.at[i, b], rt_send.at[i, b, 3], rt_recv.at[i, b, 3], {"tp": across})
+
+    def out_rows(b, c):
+        return pl.ds(pl.multiple_of(c * rows_half + b * batch, batch), batch)
+
+    def final_b(i, b):
+        landed(rx_2.at[i, b], rt_send.at[i, b, 3], rt_recv.at[i, b, 3])
+        total = 0.5 * ((sx_2[i, b].astype(f32) + rx_2[i, b].astype(f32)) * scales(i)[0:1, :])
+        cols = owner_cols(i)
+        out[out_rows(b, core), cols] = (r2[b * batch:(b + 1) * batch, cols] + total).astype(bf16)
+        done = out.at[out_rows(b, core), cols]
+        remote(done, done, rt_send.at[i, b, 4], rt_recv.at[i, b, 4], {"tp": mate})
+
+    for b in range(BATCHES):
+        if b == 0:
+            for q in range(BATCHES):
+                fold_a(n - 1, q)
+        gather_a(n - 1, b)
+        mixer(b)
+        send_third(b)
+    have_own(0)
+    hidden_rows(0, 0)
     forward_third(0)
+    have_own(1)
+    hidden_rows(1, 0)
+    forward_third(1)
+    pass_third(0)
     for i in range(n):
-        down(i, 0, 0)
-        remote(stage.at[i, 0, half_of(1 - core), :], ra_2.at[i, 0], rs_send.at[1, i, 0], rs_recv.at[1, i, 0], {"tp": mate})
-        if i + 1 < CHUNKS:
-            forward_third(i + 1)
-    for j in range(CHUNKS):
-        pass_third(j)
-    for j in range(CHUNKS):
-        landed(third.at[beside(1 - core, chip), chunk[j]], ag_send.at[j, 3], ag_recv.at[j, 3])
-        landed(third.at[beside(1 - core, 1 - chip), chunk[j]], ag_send.at[j, 4], ag_recv.at[j, 4])
-    hidden_rows(1)
-
-    def cross_b(i):
-        cross_one(i, half_of, ra_2, sz_2, rz_2, 1)
-
-    def fold_b(i):
-        fold_one(i, half_of, ra_2, rz_2, sx_2, rx_2, 1)
-
-    def final_b(i):
-        total = total_of(i, sx_2, rx_2, 1)
-        cols = owner_cols(i)
-        out[half_of(core), cols] = (r2[:, cols] + total).astype(bf16)
-        done = out.at[half_of(core), cols]
-        remote(done, done, ag_send.at[i, 5], ag_recv.at[i, 5], {"tp": mate})
-
+        down_send(i, 0, 0)
+    have_partner(0)
+    hidden_rows(0, 1)
     for i in range(n):
-        down(i, 1, 0)
-        remote(stage.at[i, 1, half_of(1 - core), :], ra_2.at[i, 1], rs_send.at[1, i, 1], rs_recv.at[1, i, 1], {"tp": mate})
-        if i > 0:
-            cross_b(i - 1)
-    cross_b(n - 1)
+        down_send(i, 0, 1)
+    pass_third(1)
     for i in range(n):
-        fold_b(i)
-        if i > 0:
-            final_b(i - 1)
-    final_b(n - 1)
+        cross_b(i, 0)
     for i in range(n):
-        landed(out.at[half_of(1 - core), owner_cols(i)], ag_send.at[i, 5], ag_recv.at[i, 5])
+        down_send(i, 1, 0)
+    have_partner(1)
+    hidden_rows(1, 1)
+    for i in range(n):
+        down_send(i, 1, 1)
+    fold_b(0, 0)
+    for i in range(n):
+        cross_b(i, 1)
+        if i + 1 < n:
+            fold_b(i + 1, 0)
+            final_b(i, 0)
+    fold_b(0, 1)
+    final_b(n - 1, 0)
+    for i in range(n):
+        if i + 1 < n:
+            fold_b(i + 1, 1)
+        final_b(i, 1)
+    for b in range(BATCHES):
+        for i in range(n):
+            landed(out.at[out_rows(b, 1 - core), owner_cols(i)], rt_send.at[i, b, 4], rt_recv.at[i, b, 4])
     wait_sent()
 
 
@@ -645,6 +689,7 @@
     groups, gc, _ = pool_map.shape
     rows_half = seq // 2
     window = rows_half + widest
+    batch = rows_half // BATCHES
     vmem = pl.BlockSpec(memory_space=pltpu.VMEM)
     dma = pltpu.SemaphoreType.DMA
     hbm = pl.BlockSpec(memory_space=pl.ANY)
@@ -655,7 +700,7 @@
     )
     return pl.pallas_call(
         functools.partial(layer_kernel, n),
-        out_shape=jax.ShapeDtypeStruct((seq, width), bf16),
+        out_shape=pltpu.VMEM((seq, width), bf16),
         in_specs=[spec for _, spec in args],
         out_specs=vmem,
         scratch_shapes=[
@@ -684,25 +729,27 @@
             pltpu.VMEM((n, window, slab), bf16),
             pltpu.VMEM((n, window, slab), bf16),
             pltpu.VMEM((window, width), f32),
-            pltpu.VMEM((window, width), bf16),
-            pltpu.VMEM((rows_half, groups * gc), bf16),
+            pltpu.VMEM((batch + widest, width), bf16),
+            pltpu.VMEM((batch, groups * gc), bf16),
             pltpu.VMEM((rows_half, width), f32),
             pltpu.VMEM((2 * seq, width), bf16),
-            pltpu.VMEM((n, 2, rows_half, slab), bf16),
-            pltpu.VMEM((n, rows_half, slab), bf16),
-            pltpu.VMEM((n, rows_half, slab), bf16),
-            pltpu.VMEM((n, rows_half, slab), bf16),
-            pltpu.VMEM((n, rows_half, slab), bf16),
+            pltpu.VMEM((n, 2 * seq, slab), bf16),
+            pltpu.VMEM((n, BATCHES, 2, batch, slab), bf16),
+            pltpu.VMEM((n, BATCHES, batch, slab), bf16),
+            pltpu.VMEM((n, BATCHES, batch, slab), bf16),
+            pltpu.VMEM((n, BATCHES, batch, slab), bf16),
+            pltpu.VMEM((n, BATCHES, batch, slab), bf16),
             dma((n - 1, FIRST_PART[-1])), dma((2, n, FIRST_PART[-1])), dma((n, 2 * FIRST_PART[-1])),
             dma((n - 1,)), dma((n,)),
             dma((3, n, 3)), dma((3, n, 3)),
             dma((4,)), dma((4,)),
-            dma((2, n, 4)), dma((2, n, 4)),
-            dma((n, 6)), dma((n, 6)),
+            dma((BATCHES, n, 4)), dma((BATCHES, n, 4)),
+            dma((n, BATCHES, 5)), dma((n, BATCHES, 5)),
+            dma((BATCHES, 5)), dma((BATCHES, 5)),
             dma((7,)),
         ],
         compiler_params=pltpu.CompilerParams(
-            collective_id=0, has_side_effects=True, vmem_limit_bytes=60 * 1024 * 1024
+            collective_id=0, has_side_effects=True, vmem_limit_bytes=62 * 1024 * 1024
         ),
     )(*[value for value, _ in args])
 

time: 140 us -> 136 us (0.971)
    pallas_call x1, Pallas kernels: 136 us -> 135 us  [fused_layer(): pl.pallas_call(functools.partial(layer_kernel, n), out_shape=pltpu.VMEM((...]
where the time goes in v2:
time: 136 us
  Pallas kernels  135 us (99%)
    pallas_call x1, Pallas kernels, fused_layer(): pl.pallas_call(functools.partial(layer_kernel, n), out_shape=pltpu.VMEM((...  135 us

profile of v2, /device:TPU:1, one launch (start us, length us, event | category | flops | bytes accessed | tf_op | source)
XLA Modules:
  0.0 135.6 jit_solution(7094871535474559285)
XLA Ops:
  0.0 134.6 %shard_map.127 = bf16[256,2048]{1,0:T(8,128)(2,1)S(1)} custom-call(bf16[256,2048]{1,0:T(8,128)(2,1)} %tok.1, f32[3,2048]{1,0:T(4,128)} %gains.1, f32[512,768]{1,0:T(8,128)} %gate_hbm.1, f32[512,768]{1,0:T(8,128)} %up_hbm.1, f32[2,768]{1,0:T(2,128)} %hs.1, f32[768,512]{1,0:T(8,128)} %down_hbm.1, f32[512,512]{1,0:T(8,128)} %mix_in_hbm.1, ...), custom_call_target="tpu_custom_call" | custom-call | tf_op jit(solution)/shard_map/pallas_call | solution.py:701
  134.6 1.0 copy.15

commit v3 on v2

--- a/solution.py
+++ b/solution.py
@@ -144,7 +144,7 @@
 FIRST_PART = (0, 1, 2, 6, 10)
 TILE = 256
 BATCHES = 2
-MIXER_AFTER = 1
+MIXER_AFTER = 2
 bf16 = jnp.bfloat16
 f32 = jnp.float32
 
@@ -304,7 +304,7 @@
     loads[3].wait()
     for u in range(PARTS[GU]):
         cast_gate_up(rep * half + u * (half // PARTS[GU]), half // PARTS[GU], (0, 1))
-        for i in (3, 2, 1):
+        for i in (1, 2, 3):
             send_own(GU, i, u)
         if u == MIXER_AFTER:
             for t in (WI, WO):
@@ -420,12 +420,12 @@
         if u == 1:
             for k in (1, 2, 3):
                 landed(ptok.at[my_rows(peers[k]), :], tk_send.at[k], tk_recv.at[k])
+            for i in (1, 2, 3):
+                for v in range(PARTS[DN]):
+                    send_own(DN, i, v, middle if i == 3 else None)
             norm_first(ptok, seq)
         if u == 2:
             relay_mixer(1)
-            for i in (1, 2, 3):
-                for v in range(PARTS[DN]):
-                    send_own(DN, i, v, middle if i == 3 else None)
             gate_up(0, True)
     relay_mixer(2)
     relay_mixer(3)
@@ -654,18 +654,21 @@
     pass_third(1)
     for i in range(n):
         cross_b(i, 0)
+    have_partner(1)
+    hidden_rows(1, 1)
+    fold_b(0, 0)
+    for i in range(n):
+        down_send(i, 1, 1)
+    fold_b(1, 0)
+    for i in range(n):
+        cross_b(i, 1)
+    fold_b(2, 0)
+    final_b(0, 0)
     for i in range(n):
         down_send(i, 1, 0)
-    have_partner(1)
-    hidden_rows(1, 1)
-    for i in range(n):
-        down_send(i, 1, 1)
-    fold_b(0, 0)
-    for i in range(n):
-        cross_b(i, 1)
-        if i + 1 < n:
-            fold_b(i + 1, 0)
-            final_b(i, 0)
+    fold_b(3, 0)
+    final_b(1, 0)
+    final_b(2, 0)
     fold_b(0, 1)
     final_b(n - 1, 0)
     for i in range(n):

time: 136 us -> 132 us (0.971)
  Pallas kernels: 135 us -> 131 us
    pallas_call x1, Pallas kernels: 135 us -> 131 us  [fused_layer(): pl.pallas_call(functools.partial(layer_kernel, n), out_shape=pltpu.VMEM((...]
where the time goes in v3:
time: 132 us
  Pallas kernels  131 us (99%)
    pallas_call x1, Pallas kernels, fused_layer(): pl.pallas_call(functools.partial(layer_kernel, n), out_shape=pltpu.VMEM((...  131 us

profile of v3, /device:TPU:1, one launch (start us, length us, event | category | flops | bytes accessed | tf_op | source)
XLA Modules:
  0.0 132.1 jit_solution(14743104129664445665)
XLA Ops:
  0.0 131.1 %shard_map.127 = bf16[256,2048]{1,0:T(8,128)(2,1)S(1)} custom-call(bf16[256,2048]{1,0:T(8,128)(2,1)} %tok.1, f32[3,2048]{1,0:T(4,128)} %gains.1, f32[512,768]{1,0:T(8,128)} %gate_hbm.1, f32[512,768]{1,0:T(8,128)} %up_hbm.1, f32[2,768]{1,0:T(2,128)} %hs.1, f32[768,512]{1,0:T(8,128)} %down_hbm.1, f32[512,512]{1,0:T(8,128)} %mix_in_hbm.1, ...), custom_call_target="tpu_custom_call" | custom-call | tf_op jit(solution)/shard_map/pallas_call | solution.py:704
  131.1 1.0 copy.15

commit v4 on v3

--- a/solution.py
+++ b/solution.py
@@ -140,8 +140,8 @@
 
 
 MESH = pl.DeviceIdType.MESH
-PARTS = (1, 1, 4, 4)
-FIRST_PART = (0, 1, 2, 6, 10)
+PARTS = (1, 1, 4, 2)
+FIRST_PART = (0, 1, 2, 6, 8)
 TILE = 256
 BATCHES = 2
 MIXER_AFTER = 2
@@ -154,8 +154,8 @@
 
 
 def layer_kernel(
-    n, tok, gains, gate_hbm, up_hbm, hs, down_hbm, mix_in_hbm, mix_out_hbm, isc, pmap, pool_scale, down_scale, out_scale,
-    out, wide_gate, wide_up, wide_down, wide_in, wide_out, sc_in, gu_own, dn_own, gu_buf, dn_buf, wi_all, wo_all, sc_all, ps_all,
+    n, tok_hbm, gains, gate_hbm, up_hbm, hs, down_hbm, mix_in_hbm, mix_out_hbm, isc, pmap_hbm, pool_scale, down_scale, out_scale,
+    out, tok, pmap, wide_gate, wide_up, wide_down, wide_in, wide_out, sc_in, gu_own, dn_own, gu_buf, dn_buf, wi_all, wo_all, sc_all, ps_all,
     ptok, first, gacc, hidden, stage, rs_a, s_z, rs_z, s_x, rs_x, r1, second, pool, r2, third, stage_2, ra_2, sz_2, rz_2, sx_2, rx_2,
     z_send, y_send, w_recv, sc_send, sc_recv, tp_send, tp_recv, tk_send, tk_recv, rs_send, rs_recv, rt_send, rt_recv, ag_send, ag_recv, loc,
 ):
@@ -198,7 +198,9 @@
         pltpu.make_async_copy(up_hbm.at[mine_half, :], wide_up.at[mine_half, :], loc.at[3]),
         pltpu.make_async_copy(gate_hbm.at[other_half, :], wide_gate.at[other_half, :], loc.at[4]),
         pltpu.make_async_copy(up_hbm.at[other_half, :], wide_up.at[other_half, :], loc.at[5]),
+        pltpu.make_async_copy(tok_hbm, tok, loc.at[7]),
         pltpu.make_async_copy(down_hbm, wide_down, loc.at[6]),
+        pltpu.make_async_copy(pmap_hbm, pmap, loc.at[8]),
     ]
     for load in loads:
         load.start()
@@ -299,6 +301,7 @@
         return pl.ds(pl.multiple_of(rank * share, share), share)
 
     pl.semaphore_wait(barrier, n - 1 + 4)
+    loads[6].wait()
     remote(tok.at[my_rows(me), :], ptok.at[my_rows(me), :], tk_send.at[0], tk_recv.at[0], {"fs": partner})
     loads[2].wait()
     loads[3].wait()
@@ -335,7 +338,8 @@
     loads[4].wait()
     loads[5].wait()
     cast_gate_up((1 - rep) * half, half, (kind,))
-    loads[6].wait()
+    loads[7].wait()
+    loads[8].wait()
 
     @pl.loop(0, hu // 32)
     def _(j):
@@ -528,12 +532,6 @@
     gather_a(0)
     fold_a(2)
     gather_a(1)
-    for k in (1, 2, 3):
-        landed(ps_all.at[peers[k]], tp_send.at[2, 0, k - 1], tp_recv.at[2, 0, k - 1])
-    for i in range(n):
-        have_mixer(i)
-    gather_a(2)
-
     def mixer(b):
         low = b * batch
         taken = slice(low, low + batch + halo)
@@ -635,6 +633,11 @@
         if b == 0:
             for q in range(BATCHES):
                 fold_a(n - 1, q)
+            gather_a(2)
+            for k in (1, 2, 3):
+                landed(ps_all.at[peers[k]], tp_send.at[2, 0, k - 1], tp_recv.at[2, 0, k - 1])
+            for i in range(n):
+                have_mixer(i)
         gather_a(n - 1, b)
         mixer(b)
         send_third(b)
@@ -697,8 +700,8 @@
     dma = pltpu.SemaphoreType.DMA
     hbm = pl.BlockSpec(memory_space=pl.ANY)
     args = (
-        (tokens, vmem), (norm_gains, vmem), (gate_weight, hbm), (up_weight, hbm), (hidden_scales, vmem),
-        (down_weight, hbm), (mix_in, hbm), (mix_out, hbm), (in_scale[None], vmem), (pool_map, vmem),
+        (tokens, hbm), (norm_gains, vmem), (gate_weight, hbm), (up_weight, hbm), (hidden_scales, vmem),
+        (down_weight, hbm), (mix_in, hbm), (mix_out, hbm), (in_scale[None], vmem), (pool_map, hbm),
         (pool_scale[None], vmem), (down_scale[None], vmem), (out_scale[None], vmem),
     )
     return pl.pallas_call(
@@ -707,6 +710,8 @@
         in_specs=[spec for _, spec in args],
         out_specs=vmem,
         scratch_shapes=[
+            pltpu.VMEM((seq, width), bf16),
+            pltpu.VMEM(pool_map.shape, f32),
             pltpu.VMEM((slab, units), f32),
             pltpu.VMEM((slab, units), f32),
             pltpu.VMEM((units, slab), f32),
@@ -749,7 +754,7 @@
             dma((BATCHES, n, 4)), dma((BATCHES, n, 4)),
             dma((n, BATCHES, 5)), dma((n, BATCHES, 5)),
             dma((BATCHES, 5)), dma((BATCHES, 5)),
-            dma((7,)),
+            dma((9,)),
         ],
         compiler_params=pltpu.CompilerParams(
             collective_id=0, has_side_effects=True, vmem_limit_bytes=62 * 1024 * 1024

time: 132 us -> 131 us (level)
    pallas_call x1, Pallas kernels: 131 us -> 130 us  [fused_layer(): pl.pallas_call(functools.partial(layer_kernel, n), out_shape=pltpu.VMEM((...]
where the time goes in v4:
time: 131 us
  Pallas kernels  130 us (99%)
    pallas_call x1, Pallas kernels, fused_layer(): pl.pallas_call(functools.partial(layer_kernel, n), out_shape=pltpu.VMEM((...  130 us

profile of v4, /device:TPU:1, one launch (start us, length us, event | category | flops | bytes accessed | tf_op | source)
XLA Modules:
  0.0 130.6 jit_solution(6933618069298928683)
XLA Ops:
  0.0 129.6 %shard_map.127 = bf16[256,2048]{1,0:T(8,128)(2,1)S(1)} custom-call(bf16[256,2048]{1,0:T(8,128)(2,1)} %tok_hbm.1, f32[3,2048]{1,0:T(4,128)} %gains.1, f32[512,768]{1,0:T(8,128)} %gate_hbm.1, f32[512,768]{1,0:T(8,128)} %up_hbm.1, f32[2,768]{1,0:T(2,128)} %hs.1, f32[768,512]{1,0:T(8,128)} %down_hbm.1, f32[512,512]{1,0:T(8,128)} %mix_in_hbm.1, ...), custom_call_target="tpu_custom_call" | custom-call | tf_op jit(solution)/shard_map/pallas_call | solution.py:707
  129.6 1.0 copy.15
